TPU v7x, 32 devices: a whole 2x2x4 slice. The times are simulated.
32 devices in a mesh: sp: 8 (over z, x), tp: 4 (over y, core).
Axes of the slice: x: 2, y: 2, z: 4, core: 2. Of those that a mesh axis runs over, the one named last changes fastest.
Arguments:
- query_logits: bfloat16 [4096, 4096], P('sp', 'tp'), may hold values from -6 to 6
- forget_logits: bfloat16 [4096, 4096], P('sp', 'tp'), may hold values from -6 to 6
- value_inputs: bfloat16 [4096, 4096], P('sp', 'tp'), may hold values from -16 to 16
- output_gate_logits: bfloat16 [4096, 4096], P('sp', 'tp'), may hold values from -6 to 6
- forget_floor_gap: float32 [4096], replicated, may hold values from 2.4414063e-05 to 0.1
- surge_log_decay: float32 [32, 4096], P('tp', 'sp'), may hold values from -0.7 to 0
- head_norm_gain: float32 [128], replicated, may hold values from 0.1 to 1.9
- output_matrix: bfloat16 [4096, 4096], P('sp', 'tp'), may hold values from -1.25 to 1.25
- branch_norm_gain: float32 [4096], replicated, may hold values from 0.1 to 1.9
- residual: bfloat16 [4096, 4096], P('sp', 'tp'), may hold values from -6 to 6
Outputs:
- output: bfloat16 [4096, 4096], P('sp', 'tp')
All inputs are finite; a program needn't handle non-finite values.
Results may differ from a plain program's by a relative error of at most 0.005.
Values may be sent and summed in bfloat16 or wider, within the bound.
A program may use at most 128 MiB of HBM per device.

v0:
```python
import jax
import jax.numpy as jnp
from jax import lax
from jax.sharding import PartitionSpec as P

HEAD_DIM = 128
D = 4096
BLOCK_SPAN = 64


epsilon = 1e-06


def prefix(shard, axis, combine, identity):
    size, position = (lax.axis_size(axis), lax.axis_index(axis))
    everything = jax.tree.map(lambda part: lax.all_gather(part, axis), shard)
    start = jax.tree.map(
        lambda part, zero: jnp.broadcast_to(jnp.asarray(zero, part.dtype), part.shape),
        shard,
        identity,
    )

    def step(k, before):
        reached = k < position
        new = combine(before, jax.tree.map(lambda part: part[k], everything))
        return jax.tree.map(lambda a, b: jnp.where(reached, a, b), new, before)

    return lax.fori_loop(0, size, step, start)


def block_update(state, queries, keys_in, values_in, running):
    length = running.shape[1]
    middle = length // 2
    anchor = running[:, middle - 1 : middle, :]
    ending = running[:, -1:, :]
    causal = jnp.tril(jnp.ones((length, length), dtype=bool))
    highest = lax.Precision.HIGHEST
    inter = jnp.einsum("htd,hde->hte", queries * jnp.exp(running), state, precision=highest)
    scores = jnp.einsum(
        "htd,hsd->hts",
        queries * jnp.exp(running - anchor),
        keys_in * jnp.exp(anchor - running),
        precision=highest,
    )
    intra = jnp.einsum(
        "hts,hse->hte", jnp.where(causal[None], scores, 0.0), values_in, precision=highest
    )
    new_state = state * jnp.exp(ending[:, 0, :])[:, :, None] + jnp.einsum(
        "hsd,hse->hde", keys_in * jnp.exp(ending - running), values_in, precision=highest
    )
    return (new_state, inter + intra)


def head_gates(query_logits, forget_logits, value_inputs, gap):
    row_count = query_logits.shape[0]
    head_count = query_logits.shape[1] // HEAD_DIM

    def shaped(array):
        return array.astype(jnp.float32).reshape(row_count, head_count, HEAD_DIM)

    queries = jax.nn.silu(shaped(query_logits)) * HEAD_DIM ** (-0.5)
    keys_in = gap.reshape(head_count, HEAD_DIM) * jax.nn.sigmoid(-shaped(forget_logits))
    values_in = shaped(value_inputs)
    decay_factors = jnp.log1p(-keys_in)
    return (queries, keys_in, values_in, decay_factors)


def gated_norm(heads_out, output_gate_logits, head_norm_gain):
    mean_sq = jnp.mean(heads_out * heads_out, axis=-1, keepdims=True)
    gates = jax.nn.silu(output_gate_logits.astype(jnp.float32).reshape(heads_out.shape))
    normed = heads_out * lax.rsqrt(mean_sq + epsilon) * head_norm_gain * gates
    return normed.reshape(heads_out.shape[0], -1).astype(jnp.bfloat16)


def combine(earlier, later):
    return (earlier[0] * later[0], later[0][:, :, None] * earlier[1] + later[1])


def per_device(
    query_logits,
    forget_logits,
    value_inputs,
    output_gate_logits,
    forget_floor_gap,
    surge_log_decay,
    head_norm_gain,
    output_matrix,
    branch_norm_gain,
    residual,
):
    row_count = query_logits.shape[0]
    head_cols = query_logits.shape[1]
    head_count = head_cols // HEAD_DIM
    number_of_blocks = row_count // BLOCK_SPAN
    column = lax.axis_index("tp")
    whole_weight = lax.all_gather(output_matrix, "sp", axis=0, tiled=True)
    gap = lax.dynamic_slice_in_dim(forget_floor_gap, column * head_cols, head_cols)
    queries, keys_in, values_in, decay_factors = head_gates(
        query_logits, forget_logits, value_inputs, gap
    )
    decay_factors = decay_factors + jnp.transpose(surge_log_decay)[:, :, None]

    def to_blocks(array):
        return array.reshape(number_of_blocks, BLOCK_SPAN, head_count, HEAD_DIM).transpose(
            0, 2, 1, 3
        )

    queries = to_blocks(queries)
    running = jnp.cumsum(to_blocks(decay_factors), axis=2)

    def step_forward(state, input_tuple):
        return block_update(state, input_tuple[0], input_tuple[1], input_tuple[2], input_tuple[3])

    starting_state = jnp.zeros((head_count, HEAD_DIM, HEAD_DIM), jnp.float32)
    end_state, local_out = lax.scan(
        step_forward, starting_state, (queries, to_blocks(keys_in), to_blocks(values_in), running)
    )
    totals = running[:, :, -1, :]
    before = jnp.cumsum(totals, axis=0) - totals
    whole_decay = jnp.exp(jnp.sum(totals, axis=0))
    identity = (jnp.ones_like(whole_decay), jnp.zeros_like(end_state))
    unused_slot, carried = prefix((whole_decay, end_state), "sp", combine, identity)
    reach = queries * jnp.exp(running + before[:, :, None, :])
    heads_out = local_out + jnp.einsum(
        "nhtd,hde->nhte", reach, carried, precision=lax.Precision.HIGHEST
    )
    heads_out = heads_out.transpose(0, 2, 1, 3).reshape(row_count, head_count, HEAD_DIM)
    mixed_rows = gated_norm(heads_out, output_gate_logits, head_norm_gain)
    all_heads = lax.all_gather(mixed_rows, "tp", axis=1, tiled=True)
    projected = jnp.dot(all_heads, whole_weight, preferred_element_type=jnp.float32)
    branch = lax.optimization_barrier(projected.astype(jnp.bfloat16)).astype(jnp.float32)
    squares = lax.psum(jnp.sum(branch * branch, axis=1), "tp")
    scale = lax.rsqrt(squares / D + epsilon)
    out_cols = branch.shape[1]
    gain_part = lax.dynamic_slice_in_dim(branch_norm_gain, column * out_cols, out_cols)
    return (residual.astype(jnp.float32) + branch * scale[:, None] * gain_part).astype(jnp.bfloat16)


def solution(mesh):
    placed = (
        P("sp", "tp"),
        P("sp", "tp"),
        P("sp", "tp"),
        P("sp", "tp"),
        P(),
        P("tp", "sp"),
        P(),
        P("sp", "tp"),
        P(),
        P("sp", "tp"),
    )
    return jax.shard_map(
        per_device, mesh=mesh, in_specs=placed, out_specs=P("sp", "tp"), check_vma=False
    )
```

profile of v0, /device:TPU:24, one launch (start us, length us, event | category | flops | bytes accessed | tf_op | source)
XLA Modules:
  0.0 346.1 jit_solution(4762647425927424889)
XLA Ops:
  6.5 0.8 copy.35
  7.4 1.8 divide_bitcast_fusion
  9.2 1.8 copy.48
  11.7 0.7 copy-done.4
  13.2 1.5 bitcast_bitcast_fusion
  14.6 4.0 %fusion.36 = f32[8,8,64,128]{3,1,2,0:T(8,128)} fusion(f32[8,64,8]{2,1,0:T(8,128)S(1)} %bitcast.184, f32[8,128]{1,0:T(8,128)S(1)} %dynamic-slice_bitcast_fusion.1, f32[8,64,8,128]{3,2,1,0:T(8,128)} %bitcast.177), kind=kOutput, calls=%fused_computation.60 | output fusion | flops 34603008 | bytes 4214784 | tf_op jit(solution)/shard_map/jit(cumsum)/reduce_window_sum | solution.py:109
  18.6 2.5 fusion.34
  21.1 47.1 %while.27 = (s32[]{:T(128)}, f32[8,128,128]{2,1,0:T(8,128)S(1)}, f32[8,8,64,128]{3,2,0,1:T(8,128)}, f32[8,8,64,128]{3,1,2,0:T(8,128)}, f32[8,8,64,128]{3,1,2,0:T...) while((s32[]{:T(128)}, f32[8,128,128]{2,1,0:T(8,128)S(1)}, ...), condition=%wide.region_2.3_spmd.clone, body=%wide.region_1.2_spmd.clone.sunk | while | flops 303075328 | bytes 7647356 | solution.py:115
  21.1 1.1 constant_dynamic-slice_fusion.7
  22.2 1.1 constant_dynamic-slice_fusion.6
  24.1 1.2 convolution_add_fusion.3
  25.9 1.1 fusion.74
  27.0 1.1 constant_dynamic-slice_fusion.7
  28.1 1.1 constant_dynamic-slice_fusion.6
  29.9 1.2 convolution_add_fusion.3
  31.8 1.1 fusion.74
  32.9 1.1 constant_dynamic-slice_fusion.7
  34.0 1.1 constant_dynamic-slice_fusion.6
  35.8 1.2 convolution_add_fusion.3
  37.7 1.1 fusion.74
  38.8 1.1 constant_dynamic-slice_fusion.7
  39.9 1.1 constant_dynamic-slice_fusion.6
  41.7 1.2 convolution_add_fusion.3
  43.5 1.2 fusion.74
  44.7 1.1 constant_dynamic-slice_fusion.7
  45.8 1.1 constant_dynamic-slice_fusion.6
  47.6 1.2 convolution_add_fusion.3
  49.5 1.1 fusion.74
  50.6 1.1 constant_dynamic-slice_fusion.7
  51.7 1.1 constant_dynamic-slice_fusion.6
  53.5 1.2 convolution_add_fusion.3
  55.3 1.1 fusion.74
  56.5 1.1 constant_dynamic-slice_fusion.7
  57.5 1.1 constant_dynamic-slice_fusion.6
  59.3 1.2 convolution_add_fusion.3
  61.2 1.2 fusion.74
  62.3 1.1 constant_dynamic-slice_fusion.7
  63.4 1.1 constant_dynamic-slice_fusion.6
  65.2 1.2 convolution_add_fusion.3
  67.1 1.1 fusion.74
  68.2 0.8 copy-done.1
  69.1 0.8 slice_reduce_fusion
  69.9 28.6 %all-gather = f32[64,128]{1,0:T(8,128)S(1)} all-gather(f32[8,128]{1,0:T(8,128)S(1)} %exp.52), channel_id=2, replica_groups=mesh['sp'=8,'tp'=4] {'sp'}, dimensions={0}, use_global_device_ids=true | all-gather | bytes 36864 | tf_op jit(solution)/shard_map/all_gather | solution.py:16
  98.5 0.9 fusion.47
  99.4 3.8 %exponential_multiply_fusion = f32[8,8,64,128]{3,1,2,0:T(8,128)} fusion(f32[8,8,64,128]{3,1,2,0:T(8,128)} %get-tuple-element.376, f32[8,8,128]{2,1,0:T(8,128)S(1)} %fusion.47, f32[8,64,8,128]{3,2,1,0:T(8,128)S(1)} %bitcast.176), kind=kLoop, calls=%fused_computation.67 | loop fusion | flops 3670016 | bytes 6324224 | tf_op jit(solution)/shard_map/mul | solution.py:123
  103.1 38.5 %all-gather.10.cloned.1.call-done = f32[64,128,128]{2,1,0:T(8,128)} async-done(((f32[8,128,128]{2,1,0:T(8,128)}), f32[64,128,128]{2,1,0:T(8,128)}) %all-gather.10.cloned.1.call-update) | async-done | bytes 4194320 | tf_op jit(solution)/shard_map/all_gather | solution.py:16
  141.7 11.4 %while.28 = (s32[]{:T(128)}, f32[8,128,128]{2,1,0:T(8,128)S(1)}, s32[]{:T(128)}, f32[8,8,128]{2,1,0:T(8,128)S(1)}, f32[8,8,128,128]{3,2,1,0:T(8,128)}, /*index=5*/s32[]{:T(128)}, s32[]{:T(128)}) while((s32[]{:T(128)}, f32[8,128,128]{2,1,0:T(8,128)S(1)}, s32[]{:T(128)}, f32[8,8,128]{2,1,0:T(8,128)S(1)}, ...), condition=%wide.region_5.6_spmd.clone, body=%wide.region_4.5_spmd.clone.sunk | while | flops 524292 | bytes 1585265 | solution.py:28
  141.7 1.4 fusion.75
  143.1 1.4 fusion.75
  144.5 1.4 fusion.75
  146.0 1.4 fusion.75
  147.4 1.4 fusion.75
  148.8 1.4 fusion.75
  150.2 1.4 fusion.75
  151.7 1.4 fusion.75
  153.1 4.7 %multiply_reduce_fusion = (f32[8,64,8]{1,0,2:T(8,128)S(1)}, f32[8,64,8,128]{3,1,0,2:T(8,128)S(1)}) fusion(f32[8,8,64,128]{3,2,0,1:T(8,128)} %get-tuple-element.137, f32[8,8,64,128]{3,1,2,0:T(8,128)} %exponential_multiply_fusion, f32[8,128,128]{2,1,0:T(8,128)S(1)} %get-tuple-element.139), kind=kOutput, calls=%fused_computation.66 | convolution fusion | flops 806875136 | bytes 6832128 | tf_op jit(solution)/shard_map/nhtd,hde->nhte/dot_general | solution.py:124
  157.9 1.2 copy.32
  160.3 2.2 fusion.43
  162.6 0.7 all-gather.8.cloned.1.call-update
  163.4 33.9 %all-gather.6.cloned.1.call-done = bf16[512,4096]{1,0:T(8,128)(2,1)} async-done(((bf16[512,1024]{1,0:T(8,128)(2,1)}), bf16[512,4096]{1,0:T(8,128)(2,1)}) %all-gather.6.cloned.1.call-update) | async-done | bytes 4194320 | tf_op jit(solution)/shard_map/all_gather | solution.py:129
  197.2 124.7 %all-gather.8.cloned.1.call-done = bf16[4096,1024]{1,0:T(8,128)(2,1)} async-done(((bf16[512,1024]{1,0:T(8,128)(2,1)}), bf16[4096,1024]{1,0:T(8,128)(2,1)}) %all-gather.8.cloned.1.call-update) | async-done | bytes 8388624 | tf_op jit(solution)/shard_map/all_gather | solution.py:96
  321.9 9.1 %convolution_convert_fusion = bf16[512,1024]{1,0:T(8,128)(2,1)S(1)} fusion(bf16[512,4096]{1,0:T(8,128)(2,1)} %all-gather.6.cloned.1.call-done, bf16[4096,1024]{1,0:T(8,128)(2,1)} %all-gather.8.cloned.1.call-done), kind=kOutput, calls=%fused_computation.74 | convolution fusion | flops 4295491584 | bytes 13631488 | tf_op jit(solution)/shard_map/dot_general | solution.py:130
  331.3 6.8 %psum.7 = f32[512]{0:T(512)S(1)} all-reduce(f32[512]{0:T(512)S(1)} %fusion.25), channel_id=1, replica_groups=mesh['sp'=8,'tp'=4] {'tp'}, use_global_device_ids=true, to_apply=%region_9.10 | all-reduce | flops 512 | bytes 4096 | tf_op jit(solution)/shard_map/psum | solution.py:132
  338.2 1.4 fusion.28
  (92 shorter events, 14.4 us)
Async XLA Ops:
  6.5 8.1 %copy-start = (f32[4096]{0:T(1024)S(1)}, f32[4096]{0:T(1024)}, u32[]{:S(2)}) copy-start(f32[4096]{0:T(1024)} %param.18) | copy-start | bytes 49156
  6.5 135.1 %all-gather.10.cloned.1.call-start = ((), (), s32[]{:S(2)}) async-start(), calls=%async_computation.2 | async-start | bytes 4718592 | tf_op jit(solution)/shard_map/all_gather | solution.py:16
  9.2 1.8 copy-start.3
  11.2 1.2 copy-start.4
  14.6 4.0 %copy-start.2 = (f32[64,8,8,128]{3,2,1,0:T(8,128)S(1)}, f32[64,8,8,128]{3,2,1,0:T(8,128)}, u32[]{:S(2)}) copy-start(f32[64,8,8,128]{3,2,1,0:T(8,128)} %copy.48) | copy-start | bytes 6291460
  21.1 77.3 %copy-start.7 = (f32[128]{0:T(128)S(1)}, f32[128]{0:T(128)}, u32[]{:S(2)}) copy-start(f32[128]{0:T(128)} %param.20) | copy-start | bytes 1540
  68.2 0.8 copy-start.1
  69.0 128.2 %all-gather.6.cloned.1.call-start = ((), (), s32[]{:S(2)}) async-start(), calls=%async_computation | async-start | bytes 5242880 | tf_op jit(solution)/shard_map/all_gather | solution.py:129
  159.1 1.2 copy-start.6
  162.6 159.3 %all-gather.8.cloned.1.call-start = ((), (), s32[]{:S(2)}) async-start(), calls=%async_computation.1 | async-start | bytes 9437184 | tf_op jit(solution)/shard_map/all_gather | solution.py:96
  163.3 174.9 %copy-start.5 = (bf16[512,1024]{1,0:T(8,128)(2,1)S(1)}, bf16[512,1024]{1,0:T(8,128)(2,1)}, u32[]{:S(2)}) copy-start(bf16[512,1024]{1,0:T(8,128)(2,1)} %param.23) | copy-start | bytes 3145732
  163.3 174.9 %dynamic-slice-start = ((f32[4096]{0:T(1024)}, s32[]{:T(128)}), f32[1024]{0:T(1024)S(1)}, s32[]{:S(2)}) async-start(f32[4096]{0:T(1024)} %param.22, s32[]{:T(128)} %select_n.32), calls=%async_computation.3 | async-start | bytes 8704 | tf_op jit(solution)/shard_map/dynamic_slice | solution.py:135
Sparse Core Ops, SparseCore 0:
  69.2 72.4 all-gather.9
  162.7 34.4 all-gather.5
  199.3 122.5 all-gather.7
where the time goes:
time: 350 us; the launch traced here: 346 us
  waiting for transfers between devices  198 us (57%)
  matrix products  42.7 us (12%)
  blocking collectives  35.4 us (10%)
  other arithmetic  29.2 us (8%)
  local copies, waits for them, and re-layouts  26.9 us (8%)
  between operations  13.3 us (4%)
    all_gather x1, waiting for transfers between devices, per_device(): whole_weight = lax.all_gather(output_matrix, 'sp', axis=0, tiled=True)  125 us
    all_gather x1, waiting for transfers between devices, prefix(): everything = jax.tree.map(lambda part: lax.all_gather(part, axis), shard)  38.5 us
    all_gather x1, waiting for transfers between devices, per_device(): all_heads = lax.all_gather(mixed_rows, 'tp', axis=1, tiled=True)  33.9 us
    all_gather x1, blocking collectives, prefix(): everything = jax.tree.map(lambda part: lax.all_gather(part, axis), shard)  28.6 us
    dynamic_slice x24, local copies, waits for them, and re-layouts, per_device(): lax.scan(step_forward, starting_state, (queries, to_blocks(keys_in), to_b...  17.5 us
    select_n x8, other arithmetic, step(): return jax.tree.map(lambda a, b: jnp.where(reached, a, b), new, before)  11 us
    dot_general x8, matrix products, block_update(): jnp.einsum('hsd,hse->hde', keys_in * jnp.exp(ending - running), values_in...  9.24 us
    dot_general x1, matrix products, per_device(): jnp.dot(all_heads, whole_weight, preferred_element_type=jnp.float32)  9.14 us
  transfers between devices with their start and end apart: 3, of which 3 were waited for; matrix products, arithmetic and copies ran while one was open for 2% of the time, Pallas kernels for 0%

commit v1 on v0

v1 whole, which is shorter than its diff:
```python
import functools

import jax
import jax.numpy as jnp
from jax import lax
from jax.experimental import pallas as pl
from jax.experimental.pallas import tpu as pltpu
from jax.sharding import Mesh
from jax.sharding import PartitionSpec as P

HEAD_DIM = 128
SPAN = 128
EPSILON = 1e-06
NT = (((1,), (1,)), ((), ()))
TN = (((0,), (0,)), ((), ()))
NN = (((1,), (0,)), ((), ()))


def dot(a, b, dims=NN):
    return lax.dot_general(a, b, dims, preferred_element_type=jnp.float32)


def lower_triangle():
    rows = lax.broadcasted_iota(jnp.int32, (SPAN, SPAN), 0)
    columns = lax.broadcasted_iota(jnp.int32, (SPAN, SPAN), 1)
    return rows >= columns


def decays(forget_ref, gap, surge_ref, block, causal):
    rows = pl.ds(block * SPAN, SPAN)
    logits = forget_ref[rows, :].astype(jnp.float32)
    keys = gap / (1.0 + jnp.exp(logits))
    series = keys * (1.0 / 7.0) + (1.0 / 6.0)
    for order in (5, 4, 3, 2):
        series = series * keys + (1.0 / order)
    logs = -(series * keys + 1.0) * keys
    high = logs.astype(jnp.bfloat16)
    low = (logs - high.astype(jnp.float32)).astype(jnp.bfloat16)
    ones = causal.astype(jnp.bfloat16)
    surge = surge_ref[0, :, rows]
    surged = jnp.sum(jnp.where(causal, surge, 0.0), axis=1, keepdims=True)
    return keys, dot(ones, high) + dot(ones, low) + surged


def state_kernel(forget_ref, value_ref, gap_ref, surge_ref, state_ref, total_ref):
    causal = lower_triangle()
    gap = gap_ref[0]
    state = jnp.zeros((HEAD_DIM, HEAD_DIM), jnp.float32)
    total = jnp.zeros((1, HEAD_DIM), jnp.float32)
    for block in range(forget_ref.shape[0] // SPAN):
        keys, running = decays(forget_ref, gap, surge_ref, block, causal)
        ending = running[SPAN - 1 : SPAN, :]
        kept = (keys * jnp.exp(ending - running)).astype(jnp.bfloat16)
        values = value_ref[pl.ds(block * SPAN, SPAN), :]
        state = state * jnp.exp(ending) + dot(values, kept, TN)
        total = total + ending
    state_ref[0] = state.astype(jnp.bfloat16)
    total_ref[0] = jnp.broadcast_to(total, total_ref.shape[1:])


def output_kernel(
    query_ref, forget_ref, value_ref, gate_ref, gap_ref, surge_ref, gain_ref, carried_ref, mixed_ref
):
    causal = lower_triangle()
    gap = gap_ref[0]
    gain = gain_ref[...]
    state = carried_ref[0].astype(jnp.float32)
    middle = SPAN // 2
    count = forget_ref.shape[0] // SPAN
    for block in range(count):
        rows = pl.ds(block * SPAN, SPAN)
        keys, running = decays(forget_ref, gap, surge_ref, block, causal)
        anchor = running[middle - 1 : middle, :]
        ending = running[SPAN - 1 : SPAN, :]
        logits = query_ref[rows, :].astype(jnp.float32)
        queries = logits * (HEAD_DIM**-0.5) / (1.0 + jnp.exp(-logits))
        reach = queries * jnp.exp(running - anchor)
        back = keys * jnp.exp(anchor - running)
        values = value_ref[rows, :]
        scores = dot(reach.astype(jnp.bfloat16), back.astype(jnp.bfloat16), NT)
        scores = jnp.where(causal, scores, 0.0).astype(jnp.bfloat16)
        inter = dot(
            (reach * jnp.exp(anchor)).astype(jnp.bfloat16), state.astype(jnp.bfloat16), NT
        )
        out = inter + dot(scores, values)
        if block + 1 < count:
            kept = (back * jnp.exp(ending - anchor)).astype(jnp.bfloat16)
            state = state * jnp.exp(ending) + dot(values, kept, TN)
        mean_sq = jnp.mean(out * out, axis=1, keepdims=True)
        gates = gate_ref[rows, :].astype(jnp.float32)
        gates = gates / (1.0 + jnp.exp(-gates))
        mixed_ref[rows, :] = (out * lax.rsqrt(mean_sq + EPSILON) * gain * gates).astype(
            jnp.bfloat16
        )


def heads_call(kernel, arrays, specs, out_shape, out_specs, heads, flops, name):
    moved = sum(a.size * a.dtype.itemsize for a in arrays)
    return pl.pallas_call(
        kernel,
        grid=(heads,),
        in_specs=specs,
        out_specs=out_specs,
        out_shape=out_shape,
        name=name,
        compiler_params=pltpu.CompilerParams(vmem_limit_bytes=32 * 1024 * 1024),
        cost_estimate=pl.CostEstimate(flops=flops, bytes_accessed=moved, transcendentals=0),
    )(*arrays)


def product_kernel(order_ref, *refs):
    parts, weight_ref, out_ref = refs[:-2], refs[-2], refs[-1]
    depth = parts[0].shape[1]
    total = None
    for place, part in enumerate(parts):
        start = pl.multiple_of(order_ref[place] * depth, depth)
        term = dot(part[...], weight_ref[pl.ds(start, depth), :])
        total = term if total is None else total + term
    out_ref[...] = total.astype(out_ref.dtype)


def product(order, parts, weight, dtype):
    rows, columns = parts[0].shape[0], weight.shape[1]
    tile = 256
    depth = parts[0].shape[1]
    return pl.pallas_call(
        product_kernel,
        grid_spec=pltpu.PrefetchScalarGridSpec(
            num_scalar_prefetch=1,
            grid=(columns // tile,),
            in_specs=[pl.BlockSpec((rows, depth), lambda j, o: (0, 0)) for _ in parts]
            + [pl.BlockSpec((weight.shape[0], tile), lambda j, o: (0, j))],
            out_specs=pl.BlockSpec((rows, tile), lambda j, o: (0, j)),
        ),
        out_shape=jax.ShapeDtypeStruct((rows, columns), dtype),
        name="product",
        cost_estimate=pl.CostEstimate(
            flops=2 * rows * weight.shape[0] * columns,
            bytes_accessed=2 * (weight.size + rows * weight.shape[0]),
            transcendentals=0,
        ),
    )(order, *parts, weight)


def per_device(
    tp_size,
    sp_size,
    query_logits,
    forget_logits,
    value_inputs,
    output_gate_logits,
    forget_floor_gap,
    surge_log_decay,
    head_norm_gain,
    output_matrix,
    branch_norm_gain,
    residual,
):
    rows, width = query_logits.shape
    heads = width // HEAD_DIM
    column = lax.axis_index("tp")
    pair = lax.axis_index("lo")
    place = lax.axis_index("hi") * 2 + pair
    depth_each = output_matrix.shape[0]
    weight = lax.all_gather(output_matrix, "hi", axis=0, tiled=True)
    gap = lax.dynamic_slice_in_dim(
        forget_floor_gap.reshape(-1, 1, HEAD_DIM), column * heads, heads, axis=0
    )

    by_head = pl.BlockSpec((rows, HEAD_DIM), lambda h: (0, h))
    gap_spec = pl.BlockSpec((1, 1, HEAD_DIM), lambda h: (h, 0, 0))
    surge_spec = pl.BlockSpec((1, 1, rows), lambda h: (h, 0, 0))
    state_spec = pl.BlockSpec((1, HEAD_DIM, HEAD_DIM), lambda h: (h, 0, 0))
    total_spec = pl.BlockSpec((1, 8, HEAD_DIM), lambda h: (h, 0, 0))
    surge = surge_log_decay.reshape(heads, 1, rows)
    flops = heads * rows * HEAD_DIM * 400
    state, total = heads_call(
        state_kernel,
        (forget_logits, value_inputs, gap, surge),
        [by_head, by_head, gap_spec, surge_spec],
        (
            jax.ShapeDtypeStruct((heads, HEAD_DIM, HEAD_DIM), jnp.bfloat16),
            jax.ShapeDtypeStruct((heads, 8, HEAD_DIM), jnp.float32),
        ),
        (state_spec, total_spec),
        heads,
        flops,
        "states",
    )
    total = total[:, :1, :]

    axes = ("hi", "lo")

    def shifted(array, by):
        return lax.ppermute(array, axes, [(i, i + by) for i in range(sp_size - by)])

    state, total = shifted(state, 1), shifted(total, 1)
    by = 1
    while by < sp_size - 1:
        earlier, span = shifted(state, by), shifted(total, by)
        merged = earlier.astype(jnp.float32) * jnp.exp(total) + state.astype(jnp.float32)
        state = merged.astype(jnp.bfloat16)
        total = total + span
        by *= 2

    mixed = heads_call(
        output_kernel,
        (
            query_logits,
            forget_logits,
            value_inputs,
            output_gate_logits,
            gap,
            surge,
            head_norm_gain.reshape(1, HEAD_DIM),
            state,
        ),
        [by_head] * 4
        + [gap_spec, surge_spec, pl.BlockSpec((1, HEAD_DIM), lambda h: (0, 0)), state_spec],
        jax.ShapeDtypeStruct((rows, width), jnp.bfloat16),
        by_head,
        heads,
        2 * flops,
        "outputs",
    )

    split = mixed.reshape(rows, width // (2 * depth_each), 2, depth_each)

    def of_parity(parity):
        return lax.dynamic_index_in_dim(split, parity, axis=2, keepdims=False).reshape(
            rows, width // 2
        )

    swap = [(0, 1), (1, 0)]
    own = of_parity(pair)
    other = lax.ppermute(of_parity(1 - pair), "lo", swap)
    order, own_parts, other_parts = [column], [own], [other]
    stride = tp_size // 2
    while stride >= 1:
        pattern = [(i, i ^ stride) for i in range(tp_size)]
        other_parts = other_parts + [lax.ppermute(p, "tp", pattern) for p in other_parts]
        own_parts = own_parts + [lax.ppermute(p, "tp", pattern) for p in own_parts]
        order = order + [o ^ stride for o in order]
        stride //= 2
    order = jnp.stack(order).astype(jnp.int32)
    away = product(order, other_parts, weight, jnp.bfloat16)
    arrived = lax.ppermute(away, "lo", swap)
    here = product(order, own_parts, weight, jnp.float32)
    projected = (here + arrived.astype(jnp.float32)).astype(jnp.bfloat16)
    branch = lax.optimization_barrier(projected).astype(jnp.float32)
    squares = lax.psum(jnp.sum(branch * branch, axis=1), "tp")
    columns = branch.shape[1]
    scale = lax.rsqrt(squares / (columns * tp_size) + EPSILON)
    gain_part = lax.dynamic_slice_in_dim(branch_norm_gain, column * columns, columns)
    return (residual.astype(jnp.float32) + branch * scale[:, None] * gain_part).astype(jnp.bfloat16)


def solution(mesh):
    sp_size, tp_size = mesh.shape["sp"], mesh.shape["tp"]
    paired = Mesh(mesh.devices.reshape(sp_size // 2, 2, tp_size), ("hi", "lo", "tp"))
    sp = ("hi", "lo")
    placed = (
        P(sp, "tp"),
        P(sp, "tp"),
        P(sp, "tp"),
        P(sp, "tp"),
        P(),
        P("tp", sp),
        P(),
        P(sp, "tp"),
        P(),
        P(sp, "tp"),
    )
    return jax.shard_map(
        functools.partial(per_device, tp_size, sp_size),
        mesh=paired,
        in_specs=placed,
        out_specs=P(sp, "tp"),
        check_vma=False,
    )
```

time: 350 us -> 212 us (0.61)
  waiting for transfers between devices: 198 us -> 117 us
  matrix products: 42.7 us -> 0 us
  Pallas kernels: 0 us -> 34.3 us
  blocking collectives: 35.4 us -> 5.66 us
  starting transfers between devices: 0.09 us -> 26.1 us
  other arithmetic: 29.2 us -> 4.63 us
  local copies, waits for them, and re-layouts: 26.9 us -> 9.73 us
    all_gather x3 -> x1, waiting for transfers between devices: 197 us -> 0.01 us  [per_device(): weight = lax.all_gather(output_matrix, 'hi', axis=0, tiled=True)]
    ppermute x0 -> x15, waiting for transfers between devices: none -> 116 us  [the longest x7 76.4 us: shifted(): return lax.ppermute(array, axes, [(i, i + by) for i in range(sp_size - by)])]
    dot_general x34 -> x0, matrix products: 42.7 us -> none  [the longest x8 9.24 us: block_update(): jnp.einsum('hsd,hse->hde', keys_in * jnp.exp(ending - running), values_in...]
    pallas_call x0 -> x4, Pallas kernels: none -> 34.3 us  [the longest x2 20.5 us: heads_call(): pl.pallas_call(kernel, grid=(heads,), in_specs=specs, out_specs=out_specs...]
    all_gather x1 -> x0, blocking collectives: 28.6 us -> none  [prefix(): everything = jax.tree.map(lambda part: lax.all_gather(part, axis), shard)]
    ppermute x0 -> x15, starting transfers between devices: none -> 26.1 us  [the longest x7 13 us: shifted(): return lax.ppermute(array, axes, [(i, i + by) for i in range(sp_size - by)])]
    dynamic_slice x26 -> x4, local copies, waits for them, and re-layouts: 17.5 us -> 2.18 us  [the longest x1 2.17 us: of_parity(): lax.dynamic_index_in_dim(split, parity, axis=2, keepdims=False)]
    select_n x8 -> x0, other arithmetic: 11 us -> none  [step(): return jax.tree.map(lambda a, b: jnp.where(reached, a, b), new, before)]
  transfers between devices with their start and end apart: 3 -> 16, of which waited for: 3 -> 11; matrix products, arithmetic and copies ran while one was open for 2% -> 2% of each run, Pallas kernels for 0% -> 16%
where the time goes in v1:
time: 212 us; the launch traced here: 211 us
  waiting for transfers between devices  117 us (55%)
  Pallas kernels  34.3 us (16%)
  starting transfers between devices  26.1 us (12%)
  between operations  13.7 us (6%)
  local copies, waits for them, and re-layouts  9.73 us (5%)
  blocking collectives  5.66 us (3%)
  other arithmetic  4.63 us (2%)
    ppermute x7, waiting for transfers between devices, shifted(): return lax.ppermute(array, axes, [(i, i + by) for i in range(sp_size - by)])  76.4 us
    pallas_call x2, Pallas kernels, heads_call(): pl.pallas_call(kernel, grid=(heads,), in_specs=specs, out_specs=out_specs...  20.5 us
    pallas_call x2, Pallas kernels, product(): pl.pallas_call(product_kernel, grid_spec=pltpu.PrefetchScalarGridSpec(num...  13.9 us
    ppermute x7, starting transfers between devices, shifted(): return lax.ppermute(array, axes, [(i, i + by) for i in range(sp_size - by)])  13 us
    ppermute x1, waiting for transfers between devices, per_device(): other = lax.ppermute(of_parity(1 - pair), 'lo', swap)  12.1 us
    ppermute x3, waiting for transfers between devices, per_device(): lax.ppermute(p, 'tp', pattern)  11.8 us
    ppermute x1, waiting for transfers between devices, per_device(): arrived = lax.ppermute(away, 'lo', swap)  9.71 us
    ppermute x1, starting transfers between devices, per_device(): other = lax.ppermute(of_parity(1 - pair), 'lo', swap)  8.59 us
  transfers between devices with their start and end apart: 16, of which 11 were waited for; matrix products, arithmetic and copies ran while one was open for 2% of the time, Pallas kernels for 16%

profile of v1, /device:TPU:24, one launch (start us, length us, event | category | flops | bytes accessed | tf_op | source)
XLA Modules:
  0.0 211.2 jit_solution(10856430301579676125)
XLA Ops:
  6.5 0.0 copy-start
  6.5 0.0 all-gather.2.cloned.1.call-start
  6.5 0.7 all-gather.2.cloned.1.call-update
  7.3 0.7 reshape.23.surge_ref
  8.0 0.0 copy-start.1
  8.0 1.2 copy-done.1
  9.3 1.2 copy-done.3
  10.5 8.4 %states.1 = (bf16[8,128,128]{2,1,0:T(8,128)(2,1)S(1)}, f32[8,8,128]{2,1,0:T(8,128)S(1)}) custom-call(bf16[512,1024]{1,0:T(8,128)(2,1)S(1)} %copy-done.1, bf16[512,1024]{1,0:T(8,128)(2,1)S(1)} %copy-done.3, f32[8,1,128]{2,1,0:T(1,128)S(1)} %constant_dynamic-slice_fusion.2.gap_ref, f32[8,1,512]{2,1,0:T(1,128)S(1)} %reshape.23.surge_ref), custom_call_target="tpu_custom_call" | custom-call | flops 209715200 | bytes 2117632 | tf_op jit(solution)/shard_map/states/pallas_call | solution.py:99
  18.9 3.4 %collective-permute-start = (bf16[8,128,128]{2,1,0:T(8,128)(2,1)S(1)}, bf16[8,128,128]{2,1,0:T(8,128)(2,1)S(1)}, u32[]{:S(2)}, u32[]{:S(2)}) collective-permute-start(bf16[8,128,128]{2,1,0:T(8,128)(2,1)S(1)} %get-tuple-element.7), channel_id=1, source_target_pairs={{0,4},{4,8},{8,12},{12,16},{16,20},{20,24},{24,28},{1,5},{5,9},{9,... | collective-permute-start | bytes 786440 | tf_op jit(solution)/shard_map/ppermute | solution.py:195
  22.3 23.8 %collective-permute-done = bf16[8,128,128]{2,1,0:T(8,128)(2,1)S(1)} collective-permute-done((bf16[8,128,128]{2,1,0:T(8,128)(2,1)S(1)}, bf16[8,128,128]{2,1,0:T(8,128)(2,1)S(1)}, u32[]{:S(2)}, u32[]{:S(2)}) %collective-permute-start) | collective-permute-done | bytes 262176 | tf_op jit(solution)/shard_map/ppermute | solution.py:195
  46.1 1.9 collective-permute-start.1
  48.0 1.9 collective-permute-start.2
  49.9 17.9 %collective-permute-done.2 = f32[8,1,128]{2,1,0:T(1,128)S(1)} collective-permute-done((f32[8,1,128]{2,1,0:T(1,128)S(1)}, f32[8,1,128]{2,1,0:T(1,128)S(1)}, u32[]{:S(2)}, u32[]{:S(2)}) %collective-permute-start.2) | collective-permute-done | bytes 4128 | tf_op jit(solution)/shard_map/ppermute | solution.py:195
  67.8 1.9 collective-permute-start.4
  69.7 4.7 %collective-permute-done.4 = f32[8,1,128]{2,1,0:T(1,128)S(1)} collective-permute-done((f32[8,1,128]{2,1,0:T(1,128)S(1)}, f32[8,1,128]{2,1,0:T(1,128)S(1)}, u32[]{:S(2)}, u32[]{:S(2)}) %collective-permute-start.4) | collective-permute-done | bytes 4128 | tf_op jit(solution)/shard_map/ppermute | solution.py:195
  74.5 0.0 collective-permute-done.1
  74.5 0.1 add_convert_fusion.3
  74.6 1.3 collective-permute-start.3
  75.9 17.1 %collective-permute-done.3 = bf16[8,128,128]{2,1,0:T(8,128)(2,1)S(1)} collective-permute-done((bf16[8,128,128]{2,1,0:T(8,128)(2,1)S(1)}, bf16[8,128,128]{2,1,0:T(8,128)(2,1)S(1)}, u32[]{:S(2)}, u32[]{:S(2)}) %collective-permute-start.3) | collective-permute-done | bytes 262176 | tf_op jit(solution)/shard_map/ppermute | solution.py:195
  93.0 0.1 add_convert_fusion.2
  93.1 1.3 collective-permute-start.5
  94.4 1.3 collective-permute-start.6
  95.7 4.2 %collective-permute-done.6 = f32[8,1,128]{2,1,0:T(1,128)S(1)} collective-permute-done((f32[8,1,128]{2,1,0:T(1,128)S(1)}, f32[8,1,128]{2,1,0:T(1,128)S(1)}, u32[]{:S(2)}, u32[]{:S(2)}) %collective-permute-start.6) | collective-permute-done | bytes 4128 | tf_op jit(solution)/shard_map/ppermute | solution.py:195
  99.9 8.7 %collective-permute-done.5 = bf16[8,128,128]{2,1,0:T(8,128)(2,1)S(1)} collective-permute-done((bf16[8,128,128]{2,1,0:T(8,128)(2,1)S(1)}, bf16[8,128,128]{2,1,0:T(8,128)(2,1)S(1)}, u32[]{:S(2)}, u32[]{:S(2)}) %collective-permute-start.5) | collective-permute-done | bytes 262176 | tf_op jit(solution)/shard_map/ppermute | solution.py:195
  108.6 0.1 add_convert_fusion.1.carried_ref
  108.7 0.0 copy-done.2
  108.7 0.0 copy-done.4
  108.7 0.0 copy-done.7
  108.7 0.0 copy-start.5
  108.7 1.2 copy-done.5
  109.9 1.2 copy-done.6
  111.2 12.1 %outputs.1 = bf16[512,1024]{1,0:T(8,128)(2,1)S(1)} custom-call(bf16[512,1024]{1,0:T(8,128)(2,1)S(1)} %copy-done.5, bf16[512,1024]{1,0:T(8,128)(2,1)S(1)} %copy-done.2, bf16[512,1024]{1,0:T(8,128)(2,1)S(1)} %copy-done.4, bf16[512,1024]{1,0:T(8,128)(2,1)S(1)} %copy-done.6, f32[8,1,128]{2,1,0:T(1,128)S(1)} %constant_dynamic-slice_fusion.2.gap_ref, ...), custom_call_target="tpu_custom_call" | custom-call | flops 419430400 | bytes 4477440 | tf_op jit(solution)/shard_map/outputs/pallas_call | solution.py:99
  123.2 0.8 reshape.25
  124.1 2.2 %constant_dynamic-slice_fusion = (bf16[512,1,1,512]{3,2,0,1:T(2,128)(2,1)S(1)}, bf16[512,1,1,512]{3,2,0,1:T(2,128)(2,1)S(1)}) fusion(bf16[512,1,2,512]{3,2,0,1:T(2,128)(2,1)S(1)} %reshape.25, s32[]{:T(128)S(6)} %select_n.15, s32[]{:T(128)S(6)} %select_n.14), kind=kLoop, calls=%fused_computation.14 | loop fusion | bytes 2097160 | tf_op jit(solution)/shard_map/jit(dynamic_index_in_dim)/dynamic_slice | solution.py:230
  126.2 0.1 copy.17
  126.4 8.6 %collective-permute-start.10 = (bf16[512,512]{1,0:T(8,128)(2,1)S(1)}, bf16[512,512]{1,0:T(8,128)(2,1)S(1)}, u32[]{:S(2)}, u32[]{:S(2)}) collective-permute-start(bf16[512,512]{1,0:T(8,128)(2,1)S(1)} %bitcast.28), channel_id=1, source_target_pairs={{0,4},{4,0},{1,5},{5,1},{2,6},{6,2},{3,7},{7,3},{8,12},{12,8},{9,1... | collective-permute-start | bytes 1572872 | tf_op jit(solution)/shard_map/ppermute | solution.py:236
  135.0 12.1 %collective-permute-done.10.refs_0_ = bf16[512,512]{1,0:T(8,128)(2,1)S(1)} collective-permute-done((bf16[512,512]{1,0:T(8,128)(2,1)S(1)}, bf16[512,512]{1,0:T(8,128)(2,1)S(1)}, u32[]{:S(2)}, u32[]{:S(2)}) %collective-permute-start.10) | collective-permute-done | bytes 524320 | tf_op jit(solution)/shard_map/ppermute | solution.py:236
  147.1 1.5 collective-permute-start.11
  148.6 0.0 collective-permute-start.12
  148.6 11.8 %collective-permute-done.11.refs_1_ = bf16[512,512]{1,0:T(8,128)(2,1)S(1)} collective-permute-done((bf16[512,512]{1,0:T(8,128)(2,1)S(1)}, bf16[512,512]{1,0:T(8,128)(2,1)S(1)}, u32[]{:S(2)}, u32[]{:S(2)}) %collective-permute-start.11) | collective-permute-done | bytes 524320 | tf_op jit(solution)/shard_map/ppermute | solution.py:241
  160.3 0.0 collective-permute-start.13
  160.3 0.7 pad_add_fusion.order_ref
  161.1 0.1 copy.18
  161.2 1.6 collective-permute-start.7
  162.8 0.0 collective-permute-done.12.refs_2_
  162.8 0.0 collective-permute-done.13.refs_3_
  162.8 0.0 copy-done.13
  162.8 0.0 copy-done.14
  162.8 6.8 %product.3 = bf16[512,1024]{1,0:T(8,128)(2,1)} custom-call(s32[4]{0:T(128)} %pad_add_fusion.order_ref, bf16[512,512]{1,0:T(8,128)(2,1)} %copy-done.13, bf16[512,512]{1,0:T(8,128)(2,1)} %copy-done.14, bf16[512,512]{1,0:T(8,128)(2,1)} %collective-permute-done.12.refs_2_, bf16[512,512]{1,0:T(8,128)(2,1)} %collective-permute-done.13.refs_3_, ...), custom_call_target="tpu_custom_call" | custom-call | flops 2147483648 | bytes 6291456 | tf_op jit(solution)/shard_map/product/pallas_call | solution.py:126
  169.6 1.5 collective-permute-start.14
  171.1 0.0 collective-permute-start.8
  171.1 4.4 %collective-permute-done.7.refs_1_ = bf16[512,512]{1,0:T(8,128)(2,1)S(1)} collective-permute-done((bf16[512,512]{1,0:T(8,128)(2,1)S(1)}, bf16[512,512]{1,0:T(8,128)(2,1)S(1)}, u32[]{:S(2)}, u32[]{:S(2)}) %collective-permute-start.7) | collective-permute-done | bytes 524320 | tf_op jit(solution)/shard_map/ppermute | solution.py:242
  175.5 0.0 collective-permute-start.9
  175.5 0.0 collective-permute-done.8.refs_2_
  175.5 1.9 collective-permute-done.9.refs_3_
  177.4 0.0 copy-done.11
  177.4 0.8 copy-done.12
  178.3 7.0 %product.2 = f32[512,1024]{1,0:T(8,128)} custom-call(s32[4]{0:T(128)} %pad_add_fusion.order_ref, bf16[512,512]{1,0:T(8,128)(2,1)} %bitcast.27, bf16[512,512]{1,0:T(8,128)(2,1)} %copy-done.10, bf16[512,512]{1,0:T(8,128)(2,1)} %copy-done.11, bf16[512,512]{1,0:T(8,128)(2,1)} %copy-done.12, bf16[2048,1024]{1,0:T(8,128)(2,1)} %all-gather.2.cloned.1.call-done.refs_4_), custom_call_target="tpu_custom_call" | custom-call | flops 2147483648 | bytes 6291456 | tf_op jit(solution)/shard_map/product/pallas_call | solution.py:126
  185.3 9.7 %collective-permute-done.14 = bf16[512,1024]{1,0:T(8,128)(2,1)S(1)} collective-permute-done((bf16[512,1024]{1,0:T(8,128)(2,1)}, bf16[512,1024]{1,0:T(8,128)(2,1)S(1)}, u32[]{:S(2)}, u32[]{:S(2)}) %collective-permute-start.14) | collective-permute-done | bytes 1048608 | tf_op jit(solution)/shard_map/ppermute | solution.py:247
  195.0 1.9 add_convert_fusion
  197.0 0.3 fusion
  197.3 5.7 %psum.7 = f32[512]{0:T(512)S(1)} all-reduce(f32[512]{0:T(512)S(1)} %fusion), channel_id=1, replica_groups=mesh['hi'=4,'lo'=2,'tp'=4] {'tp'}, use_global_device_ids=true, to_apply=%region_1.2 | all-reduce | flops 512 | bytes 4096 | tf_op jit(solution)/shard_map/psum | solution.py:251
  202.9 0.0 dynamic-slice-done
  203.0 1.4 fusion.3
  (23 shorter events, 0.1 us)
Async XLA Ops:
  6.5 1.5 copy-start
  6.5 156.2 %all-gather.2.cloned.1.call-start = ((), (), s32[]{:S(2)}) async-start(), calls=%async_computation | async-start | bytes 5242880 | tf_op jit(solution)/shard_map/all_gather | solution.py:165
  8.0 1.2 copy-start.1
  9.3 1.2 copy-start.3
  10.5 98.2 %copy-start.2 = (bf16[512,1024]{1,0:T(8,128)(2,1)S(1)}, bf16[512,1024]{1,0:T(8,128)(2,1)}, u32[]{:S(2)}) copy-start(bf16[512,1024]{1,0:T(8,128)(2,1)} %forget_ref.3) | copy-start | bytes 3145732
  10.5 98.2 %copy-start.4 = (bf16[512,1024]{1,0:T(8,128)(2,1)S(1)}, bf16[512,1024]{1,0:T(8,128)(2,1)}, u32[]{:S(2)}) copy-start(bf16[512,1024]{1,0:T(8,128)(2,1)} %value_ref.3) | copy-start | bytes 3145732
  10.5 98.2 %copy-start.7 = (f32[128]{0:T(128)S(1)}, f32[128]{0:T(128)}, u32[]{:S(2)}) copy-start(f32[128]{0:T(128)} %param.16) | copy-start | bytes 1540
  18.9 27.2 %collective-permute-start = (bf16[8,128,128]{2,1,0:T(8,128)(2,1)S(1)}, bf16[8,128,128]{2,1,0:T(8,128)(2,1)S(1)}, u32[]{:S(2)}, u32[]{:S(2)}) collective-permute-start(bf16[8,128,128]{2,1,0:T(8,128)(2,1)S(1)} %get-tuple-element.7), channel_id=1, source_target_pairs={{0,4},{4,8},{8,12},{12,16},{16,20},{20,24},{24,28},{1,5},{5,9},{9,... | collective-permute-start | bytes 786440 | tf_op jit(solution)/shard_map/ppermute | solution.py:195
  46.1 28.4 %collective-permute-start.1 = (bf16[8,128,128]{2,1,0:T(8,128)(2,1)S(1)}, bf16[8,128,128]{2,1,0:T(8,128)(2,1)S(1)}, u32[]{:S(2)}, u32[]{:S(2)}) collective-permute-start(bf16[8,128,128]{2,1,0:T(8,128)(2,1)S(1)} %collective-permute-done), channel_id=1, source_target_pairs={{0,4},{4,8},{8,12},{12,16},{16,20},{20,24},{24,28},{1,5},{5,9},{9,... | collective-permute-start | bytes 786440 | tf_op jit(solution)/shard_map/ppermute | solution.py:195
  48.0 19.8 %collective-permute-start.2 = (f32[8,1,128]{2,1,0:T(1,128)S(1)}, f32[8,1,128]{2,1,0:T(1,128)S(1)}, u32[]{:S(2)}, u32[]{:S(2)}) collective-permute-start(f32[8,1,128]{2,1,0:T(1,128)S(1)} %slice.3), channel_id=1, source_target_pairs={{0,4},{4,8},{8,12},{12,16},{16,20},{20,24},{24,28},{1,5},{5,9},{9,... | collective-permute-start | bytes 12296 | tf_op jit(solution)/shard_map/ppermute | solution.py:195
  67.8 6.7 %collective-permute-start.4 = (f32[8,1,128]{2,1,0:T(1,128)S(1)}, f32[8,1,128]{2,1,0:T(1,128)S(1)}, u32[]{:S(2)}, u32[]{:S(2)}) collective-permute-start(f32[8,1,128]{2,1,0:T(1,128)S(1)} %collective-permute-done.2), channel_id=1, source_target_pairs={{0,4},{4,8},{8,12},{12,16},{16,20},{20,24},{24,28},{1,5},{5,9},{9,... | collective-permute-start | bytes 12296 | tf_op jit(solution)/shard_map/ppermute | solution.py:195
  74.6 18.4 %collective-permute-start.3 = (bf16[8,128,128]{2,1,0:T(8,128)(2,1)S(1)}, bf16[8,128,128]{2,1,0:T(8,128)(2,1)S(1)}, u32[]{:S(2)}, u32[]{:S(2)}) collective-permute-start(bf16[8,128,128]{2,1,0:T(8,128)(2,1)S(1)} %add_convert_fusion.3), channel_id=1, source_target_pairs={{0,8},{4,12},{8,16},{12,20},{16,24},{20,28},{1,9},{5,13},{9,17},{1... | collective-permute-start | bytes 786440 | tf_op jit(solution)/shard_map/ppermute | solution.py:195
  93.1 15.5 %collective-permute-start.5 = (bf16[8,128,128]{2,1,0:T(8,128)(2,1)S(1)}, bf16[8,128,128]{2,1,0:T(8,128)(2,1)S(1)}, u32[]{:S(2)}, u32[]{:S(2)}) collective-permute-start(bf16[8,128,128]{2,1,0:T(8,128)(2,1)S(1)} %add_convert_fusion.2), channel_id=1, source_target_pairs={{0,16},{4,20},{8,24},{12,28},{1,17},{5,21},{9,25},{13,29},{2,18},{... | collective-permute-start | bytes 786440 | tf_op jit(solution)/shard_map/ppermute | solution.py:195
  94.4 5.5 %collective-permute-start.6 = (f32[8,1,128]{2,1,0:T(1,128)S(1)}, f32[8,1,128]{2,1,0:T(1,128)S(1)}, u32[]{:S(2)}, u32[]{:S(2)}) collective-permute-start(f32[8,1,128]{2,1,0:T(1,128)S(1)} %bitcast.32), channel_id=1, source_target_pairs={{0,8},{4,12},{8,16},{12,20},{16,24},{20,28},{1,9},{5,13},{9,17},{1... | collective-permute-start | bytes 12296 | tf_op jit(solution)/shard_map/ppermute | solution.py:195
  108.7 1.2 copy-start.5
  109.9 1.2 copy-start.6
  126.4 20.7 %collective-permute-start.10 = (bf16[512,512]{1,0:T(8,128)(2,1)S(1)}, bf16[512,512]{1,0:T(8,128)(2,1)S(1)}, u32[]{:S(2)}, u32[]{:S(2)}) collective-permute-start(bf16[512,512]{1,0:T(8,128)(2,1)S(1)} %bitcast.28), channel_id=1, source_target_pairs={{0,4},{4,0},{1,5},{5,1},{2,6},{6,2},{3,7},{7,3},{8,12},{12,8},{9,1... | collective-permute-start | bytes 1572872 | tf_op jit(solution)/shard_map/ppermute | solution.py:236
  147.1 15.7 %copy-start.13 = (bf16[512,512]{1,0:T(8,128)(2,1)}, bf16[512,512]{1,0:T(8,128)(2,1)S(1)}, u32[]{:S(2)}) copy-start(bf16[512,512]{1,0:T(8,128)(2,1)S(1)} %collective-permute-done.10.refs_0_) | copy-start | bytes 1572868
  147.1 13.3 %collective-permute-start.11 = (bf16[512,512]{1,0:T(8,128)(2,1)S(1)}, bf16[512,512]{1,0:T(8,128)(2,1)S(1)}, u32[]{:S(2)}, u32[]{:S(2)}) collective-permute-start(bf16[512,512]{1,0:T(8,128)(2,1)S(1)} %collective-permute-done.10.refs_0_), channel_id=1, source_target_pairs={{0,2},{1,3},{2,0},{3,1},{4,6},{5,7},{6,4},{7,5},{8,10},{9,11},{10,... | collective-permute-start | bytes 1572872 | tf_op jit(solution)/shard_map/ppermute | solution.py:241
  148.6 14.2 %collective-permute-start.12 = (bf16[512,512]{1,0:T(8,128)(2,1)S(1)}, bf16[512,512]{1,0:T(8,128)(2,1)}, u32[]{:S(2)}, u32[]{:S(2)}) collective-permute-start(bf16[512,512]{1,0:T(8,128)(2,1)S(1)} %collective-permute-done.10.refs_0_), channel_id=1, source_target_pairs={{0,1},{1,0},{2,3},{3,2},{4,5},{5,4},{6,7},{7,6},{8,9},{9,8},{10,11... | collective-permute-start | bytes 1572872 | tf_op jit(solution)/shard_map/ppermute | solution.py:241
  160.3 2.4 %copy-start.14 = (bf16[512,512]{1,0:T(8,128)(2,1)}, bf16[512,512]{1,0:T(8,128)(2,1)S(1)}, u32[]{:S(2)}) copy-start(bf16[512,512]{1,0:T(8,128)(2,1)S(1)} %collective-permute-done.11.refs_1_) | copy-start | bytes 1572868
  160.3 2.4 %collective-permute-start.13 = (bf16[512,512]{1,0:T(8,128)(2,1)S(1)}, bf16[512,512]{1,0:T(8,128)(2,1)}, u32[]{:S(2)}, u32[]{:S(2)}) collective-permute-start(bf16[512,512]{1,0:T(8,128)(2,1)S(1)} %collective-permute-done.11.refs_1_), channel_id=1, source_target_pairs={{0,1},{1,0},{2,3},{3,2},{4,5},{5,4},{6,7},{7,6},{8,9},{9,8},{10,11... | collective-permute-start | bytes 1572872 | tf_op jit(solution)/shard_map/ppermute | solution.py:241
  161.2 9.9 %copy-start.8 = (bf16[512,1,1,512]{3,0,2,1:T(8,128)(2,1)}, bf16[512,1,1,512]{3,0,2,1:T(8,128)(2,1)S(1)}, u32[]{:S(2)}) copy-start(bf16[512,1,1,512]{3,0,2,1:T(8,128)(2,1)S(1)} %copy.18) | copy-start | bytes 1572868
  161.2 14.3 %collective-permute-start.7 = (bf16[512,512]{1,0:T(8,128)(2,1)S(1)}, bf16[512,512]{1,0:T(8,128)(2,1)S(1)}, u32[]{:S(2)}, u32[]{:S(2)}) collective-permute-start(bf16[512,512]{1,0:T(8,128)(2,1)S(1)} %bitcast.25), channel_id=1, source_target_pairs={{0,2},{1,3},{2,0},{3,1},{4,6},{5,7},{6,4},{7,5},{8,10},{9,11},{10,... | collective-permute-start | bytes 1572872 | tf_op jit(solution)/shard_map/ppermute | solution.py:242
  169.6 25.4 %collective-permute-start.14 = (bf16[512,1024]{1,0:T(8,128)(2,1)}, bf16[512,1024]{1,0:T(8,128)(2,1)S(1)}, u32[]{:S(2)}, u32[]{:S(2)}) collective-permute-start(bf16[512,1024]{1,0:T(8,128)(2,1)} %product.3), channel_id=1, source_target_pairs={{0,4},{4,0},{1,5},{5,1},{2,6},{6,2},{3,7},{7,3},{8,12},{12,8},{9,1... | collective-permute-start | bytes 3145736 | tf_op jit(solution)/shard_map/ppermute | solution.py:247
  171.1 4.4 %collective-permute-start.8 = (bf16[512,512]{1,0:T(8,128)(2,1)S(1)}, bf16[512,512]{1,0:T(8,128)(2,1)S(1)}, u32[]{:S(2)}, u32[]{:S(2)}) collective-permute-start(bf16[512,512]{1,0:T(8,128)(2,1)S(1)} %bitcast.26), channel_id=1, source_target_pairs={{0,1},{1,0},{2,3},{3,2},{4,5},{5,4},{6,7},{7,6},{8,9},{9,8},{10,11... | collective-permute-start | bytes 1572872 | tf_op jit(solution)/shard_map/ppermute | solution.py:242
  175.5 1.9 copy-start.10
  175.5 1.9 collective-permute-start.9
  175.5 1.9 copy-start.11
  177.4 0.8 copy-start.12
  185.3 17.6 %copy-start.9 = (bf16[512,1024]{1,0:T(8,128)(2,1)S(1)}, bf16[512,1024]{1,0:T(8,128)(2,1)}, u32[]{:S(2)}) copy-start(bf16[512,1024]{1,0:T(8,128)(2,1)} %param.19) | copy-start | bytes 3145732
  185.3 17.6 %dynamic-slice-start = ((f32[4096]{0:T(1024)}, s32[]{:T(128)}), f32[1024]{0:T(1024)S(1)}, s32[]{:S(2)}) async-start(f32[4096]{0:T(1024)} %param.18, s32[]{:T(128)} %select_n.16), calls=%async_computation.1 | async-start | bytes 8704 | tf_op jit(solution)/shard_map/dynamic_slice | solution.py:254
Sparse Core Ops, SparseCore 0:
  8.9 83.6 all-gather.1

commit v2 on v1

v2 whole, which is shorter than its diff:
```python
import functools

import jax
import jax.numpy as jnp
from jax import lax
from jax.experimental import pallas as pl
from jax.experimental.pallas import tpu as pltpu
from jax.sharding import Mesh
from jax.sharding import PartitionSpec as P

HEAD_DIM = 128
SPAN = 128
EPSILON = 1e-06
NT = (((1,), (1,)), ((), ()))
TN = (((0,), (0,)), ((), ()))
NN = (((1,), (0,)), ((), ()))


def dot(a, b, dims=NN):
    return lax.dot_general(a, b, dims, preferred_element_type=jnp.float32)


def lower_triangle():
    rows = lax.broadcasted_iota(jnp.int32, (SPAN, SPAN), 0)
    columns = lax.broadcasted_iota(jnp.int32, (SPAN, SPAN), 1)
    return rows >= columns


def decays(logits, gap, surge, causal):
    keys = gap / (1.0 + jnp.exp(logits.astype(jnp.float32)))
    series = keys * (1.0 / 7.0) + (1.0 / 6.0)
    for order in (5, 4, 3, 2):
        series = series * keys + (1.0 / order)
    logs = -(series * keys + 1.0) * keys
    high = logs.astype(jnp.bfloat16)
    low = (logs - high.astype(jnp.float32)).astype(jnp.bfloat16)
    ones = causal.astype(jnp.bfloat16)
    surged = jnp.sum(jnp.where(causal, surge, 0.0), axis=1, keepdims=True)
    return keys, dot(ones, high) + dot(ones, low) + surged


def head_state(lanes, head, rows, forget_ref, value_ref, gap_ref, surge_ref):
    causal = lower_triangle()
    gap = gap_ref[head]
    state = jnp.zeros((HEAD_DIM, HEAD_DIM), jnp.float32)
    total = jnp.zeros((1, HEAD_DIM), jnp.float32)
    for start in range(0, rows, SPAN):
        span = pl.ds(start, SPAN)
        keys, running = decays(forget_ref[span, lanes], gap, surge_ref[head, :, span], causal)
        ending = running[SPAN - 1 : SPAN, :]
        kept = (keys * jnp.exp(ending - running)).astype(jnp.bfloat16)
        state = state * jnp.exp(ending) + dot(value_ref[span, lanes], kept, TN)
        total = total + ending
    return state, total


def head_output(
    lanes, head, rows, query_ref, forget_ref, value_ref, gate_ref, gap_ref, surge_ref, gain, state, put
):
    causal = lower_triangle()
    gap = gap_ref[head]
    middle = SPAN // 2
    for start in range(0, rows, SPAN):
        span = pl.ds(start, SPAN)
        keys, running = decays(forget_ref[span, lanes], gap, surge_ref[head, :, span], causal)
        anchor = running[middle - 1 : middle, :]
        ending = running[SPAN - 1 : SPAN, :]
        logits = query_ref[span, lanes].astype(jnp.float32)
        queries = logits * (HEAD_DIM**-0.5) / (1.0 + jnp.exp(-logits))
        reach = queries * jnp.exp(running - anchor)
        back = keys * jnp.exp(anchor - running)
        values = value_ref[span, lanes]
        scores = dot(reach.astype(jnp.bfloat16), back.astype(jnp.bfloat16), NT)
        scores = jnp.where(causal, scores, 0.0).astype(jnp.bfloat16)
        inter = dot(
            (reach * jnp.exp(anchor)).astype(jnp.bfloat16), state.astype(jnp.bfloat16), NT
        )
        out = inter + dot(scores, values)
        if start + SPAN < rows:
            kept = (back * jnp.exp(ending - anchor)).astype(jnp.bfloat16)
            state = state * jnp.exp(ending) + dot(values, kept, TN)
        mean_sq = jnp.mean(out * out, axis=1, keepdims=True)
        gates = gate_ref[span, lanes].astype(jnp.float32)
        gates = gates / (1.0 + jnp.exp(-gates))
        put(span, (out * lax.rsqrt(mean_sq + EPSILON) * gain * gates).astype(jnp.bfloat16))


MESH_ID = pl.DeviceIdType.MESH


def front_kernel(
    sizes,
    query_ref,
    forget_ref,
    value_ref,
    gate_ref,
    gap_ref,
    surge_ref,
    gain_ref,
    parts_ref,
    state_out,
    total_out,
    state_in,
    total_in,
    carried,
    span_total,
    away,
    state_sems,
    total_sems,
    swap_sems,
    tp_sems,
):
    hi_size, inner_size, tp_size, block = sizes
    sp_size = 2 * hi_size * inner_size
    rows, width = query_ref.shape
    heads = width // HEAD_DIM
    half = heads // 2
    per = block // HEAD_DIM
    lo, inner, tp = (lax.axis_index(a) for a in ("lo", "inner", "tp"))
    place = (lax.axis_index("hi") * 2 + lo) * inner_size + inner

    def at(position):
        return {
            "hi": position // (2 * inner_size),
            "lo": (position // inner_size) % 2,
            "inner": position % inner_size,
        }

    shifts = [1]
    by = 1
    while by < sp_size - 1:
        shifts.append(by)
        by *= 2
    strides = []
    stride = tp_size // 2
    while stride >= 1:
        strides.append(stride)
        stride //= 2

    def flipped(stride):
        return tp + stride - 2 * stride * ((tp // stride) % 2)

    barrier = pltpu.get_barrier_semaphore()
    reaches = sorted(set(shifts + [inner_size]))
    peers = len(strides)
    for by in reaches:
        for there in (place + by, place - by):
            inside = (there >= 0) & (there < sp_size)

            @pl.when(inside)
            def _():
                pl.semaphore_signal(barrier, inc=1, device_id=at(there), device_id_type=MESH_ID)

            peers = peers + jnp.where(inside, 1, 0)
    for stride in strides:
        pl.semaphore_signal(
            barrier, inc=1, device_id={"tp": flipped(stride)}, device_id_type=MESH_ID
        )
    pl.semaphore_wait(barrier, peers)

    def lanes_of(head):
        return pl.ds(pl.multiple_of(head * HEAD_DIM, HEAD_DIM), HEAD_DIM)

    def state_body(head, carry):
        state, total = head_state(
            lanes_of(head), head, rows, forget_ref, value_ref, gap_ref, surge_ref
        )
        state_out[0, head] = state.astype(jnp.bfloat16)
        total_out[0, head] = jnp.broadcast_to(total, (8, HEAD_DIM))
        return carry

    lax.fori_loop(0, heads, state_body, 0)

    for turn, by in enumerate(shifts):
        copies = [
            pltpu.make_async_remote_copy(
                src_ref=source.at[turn],
                dst_ref=target.at[turn],
                send_sem=sems.at[0, turn],
                recv_sem=sems.at[1, turn],
                device_id=at(place + by),
                device_id_type=MESH_ID,
            )
            for source, target, sems in (
                (state_out, state_in, state_sems),
                (total_out, total_in, total_sems),
            )
        ]

        @pl.when(place + by < sp_size)
        def _():
            for copy in copies:
                copy.start()

        if turn == 0:

            @pl.when(place == 0)
            def _():
                carried[...] = jnp.zeros_like(carried)
                span_total[...] = jnp.zeros_like(span_total)

        @pl.when(place - by >= 0)
        def _():
            for copy in copies:
                copy.wait_recv()

            def merge(head, carry):
                arrived = state_in[turn, head].astype(jnp.float32)
                passed = total_in[turn, head]
                if turn == 0:
                    carried[head] = arrived
                    span_total[head] = passed
                else:
                    carried[head] = arrived * jnp.exp(span_total[head, 0:1, :]) + carried[head]
                    span_total[head] = span_total[head] + passed
                return carry

            lax.fori_loop(0, heads, merge, 0)

        if turn + 1 < len(shifts):
            state_out[turn + 1] = carried[...].astype(jnp.bfloat16)
            total_out[turn + 1] = span_total[...]

    gain = gain_ref[...]

    def compute(head, put):
        head_output(
            lanes_of(head),
            head,
            rows,
            query_ref,
            forget_ref,
            value_ref,
            gate_ref,
            gap_ref,
            surge_ref,
            gain,
            carried[head],
            put,
        )

    def head_of(chunk, parity):
        return (chunk // per * 2 + parity) * per + chunk % per

    def columns(chunk):
        return pl.ds(pl.multiple_of(chunk * HEAD_DIM, HEAD_DIM), HEAD_DIM)

    def swap_copy(chunk):
        return pltpu.make_async_remote_copy(
            src_ref=away.at[:, columns(chunk)],
            dst_ref=parts_ref.at[1, tp, :, columns(chunk)],
            send_sem=swap_sems.at[0, chunk],
            recv_sem=swap_sems.at[1, chunk],
            device_id={"lo": 1 - lo},
            device_id_type=MESH_ID,
        )

    def tp_copy(stage, which, mine, chunk):
        slot = tp
        for bit, stride in enumerate(strides[:stage]):
            if (mine >> bit) & 1:
                slot = slot + stride - 2 * stride * ((tp // stride) % 2)
        return pltpu.make_async_remote_copy(
            src_ref=parts_ref.at[which, slot, :, columns(chunk)],
            dst_ref=parts_ref.at[which, slot, :, columns(chunk)],
            send_sem=tp_sems.at[0, stage, which, mine, chunk],
            recv_sem=tp_sems.at[1, stage, which, mine, chunk],
            device_id={"tp": flipped(strides[stage])},
            device_id_type=MESH_ID,
        )

    def away_body(chunk, carry):
        def put(span, value):
            away[span, columns(chunk)] = value

        compute(head_of(chunk, 1 - lo), put)
        swap_copy(chunk).start()
        return carry

    lax.fori_loop(0, half, away_body, 0)

    def own_body(chunk, carry):
        def put(span, value):
            parts_ref[0, tp, span, columns(chunk)] = value

        compute(head_of(chunk, lo), put)
        for stage in range(len(strides)):
            tp_copy(stage, 0, 0, chunk).start()
        swap_copy(chunk).wait_recv()
        for stage in range(len(strides)):
            tp_copy(stage, 1, 0, chunk).start()
        return carry

    lax.fori_loop(0, half, own_body, 0)

    for stage in range(len(strides)):

        def pass_body(chunk, carry):
            for which in (0, 1):
                for mine in range(1 << stage):
                    tp_copy(stage, which, mine, chunk).wait_recv()
                    for later in range(stage + 1, len(strides)):
                        tp_copy(later, which, mine | (1 << stage), chunk).start()
            return carry

        lax.fori_loop(0, half, pass_body, 0)

    for turn, by in enumerate(shifts):

        @pl.when(place + by < sp_size)
        def _():
            for source, target, sems in (
                (state_out, state_in, state_sems),
                (total_out, total_in, total_sems),
            ):
                pltpu.make_async_remote_copy(
                    src_ref=source.at[turn],
                    dst_ref=target.at[turn],
                    send_sem=sems.at[0, turn],
                    recv_sem=sems.at[1, turn],
                    device_id=at(place + by),
                    device_id_type=MESH_ID,
                ).wait_send()

    def sent_body(chunk, carry):
        swap_copy(chunk).wait_send()
        for stage in range(len(strides)):
            for which in (0, 1):
                for mine in range(1 << stage):
                    tp_copy(stage, which, mine, chunk).wait_send()
        return carry

    lax.fori_loop(0, half, sent_body, 0)


def front(sizes, query_logits, forget_logits, value_inputs, gate_logits, gap, surge, gain):
    hi_size, inner_size, tp_size, block = sizes
    rows, width = query_logits.shape
    heads = width // HEAD_DIM
    turns = 1 + (2 * hi_size * inner_size - 2).bit_length()
    stages = tp_size.bit_length() - 1
    vmem = pl.BlockSpec(memory_space=pltpu.VMEM)
    state = (heads, HEAD_DIM, HEAD_DIM)
    return pl.pallas_call(
        functools.partial(front_kernel, sizes),
        in_specs=[vmem] * 7,
        out_specs=vmem,
        out_shape=jax.ShapeDtypeStruct((2, tp_size, rows, width // 2), jnp.bfloat16),
        scratch_shapes=[
            pltpu.VMEM((turns,) + state, jnp.bfloat16),
            pltpu.VMEM((turns, heads, 8, HEAD_DIM), jnp.float32),
            pltpu.VMEM((turns,) + state, jnp.bfloat16),
            pltpu.VMEM((turns, heads, 8, HEAD_DIM), jnp.float32),
            pltpu.VMEM(state, jnp.float32),
            pltpu.VMEM((heads, 8, HEAD_DIM), jnp.float32),
            pltpu.VMEM((rows, width // 2), jnp.bfloat16),
            pltpu.SemaphoreType.DMA((2, turns)),
            pltpu.SemaphoreType.DMA((2, turns)),
            pltpu.SemaphoreType.DMA((2, heads // 2)),
            pltpu.SemaphoreType.DMA((2, stages, 2, tp_size // 2, heads // 2)),
        ],
        name="front",
        compiler_params=pltpu.CompilerParams(
            collective_id=0, has_side_effects=True, vmem_limit_bytes=48 * 1024 * 1024
        ),
        cost_estimate=pl.CostEstimate(
            flops=rows * width * 2000, bytes_accessed=8 * rows * width, transcendentals=0
        ),
    )(query_logits, forget_logits, value_inputs, gate_logits, gap, surge, gain)


def product_kernel(parts_ref, weight_ref, out_ref):
    depth = parts_ref.shape[-1]
    total = None
    for place in range(parts_ref.shape[1]):
        term = dot(parts_ref[0, place], weight_ref[pl.ds(place * depth, depth), :])
        total = term if total is None else total + term
    out_ref[...] = total.astype(out_ref.dtype)


def product(which, parts, weight, dtype):
    rows, columns = parts.shape[2], weight.shape[1]
    tile = 256
    return pl.pallas_call(
        product_kernel,
        grid=(columns // tile,),
        in_specs=[
            pl.BlockSpec((1,) + parts.shape[1:], lambda j: (which, 0, 0, 0)),
            pl.BlockSpec((weight.shape[0], tile), lambda j: (0, j)),
        ],
        out_specs=pl.BlockSpec((rows, tile), lambda j: (0, j)),
        out_shape=jax.ShapeDtypeStruct((rows, columns), dtype),
        name="product",
        cost_estimate=pl.CostEstimate(
            flops=2 * rows * weight.shape[0] * columns,
            bytes_accessed=2 * (weight.size + rows * weight.shape[0]),
            transcendentals=0,
        ),
    )(parts, weight)


def per_device(
    hi_size,
    inner_size,
    tp_size,
    query_logits,
    forget_logits,
    value_inputs,
    output_gate_logits,
    forget_floor_gap,
    surge_log_decay,
    head_norm_gain,
    output_matrix,
    branch_norm_gain,
    residual,
):
    rows, width = query_logits.shape
    heads = width // HEAD_DIM
    column = lax.axis_index("tp")
    weight = lax.all_gather(output_matrix, ("hi", "inner"), axis=0, tiled=True)
    gap = lax.dynamic_slice_in_dim(
        forget_floor_gap.reshape(-1, 1, HEAD_DIM), column * heads, heads, axis=0
    )
    parts = front(
        (hi_size, inner_size, tp_size, inner_size * output_matrix.shape[0]),
        query_logits,
        forget_logits,
        value_inputs,
        output_gate_logits,
        gap,
        surge_log_decay.reshape(heads, 1, rows),
        head_norm_gain.reshape(1, HEAD_DIM),
    )
    away = product(1, parts, weight, jnp.bfloat16)
    arrived = lax.ppermute(away, "lo", [(0, 1), (1, 0)])
    here = product(0, parts, weight, jnp.float32)
    projected = (here + arrived.astype(jnp.float32)).astype(jnp.bfloat16)
    branch = lax.optimization_barrier(projected).astype(jnp.float32)
    squares = lax.psum(jnp.sum(branch * branch, axis=1), "tp")
    columns = branch.shape[1]
    scale = lax.rsqrt(squares / (columns * tp_size) + EPSILON)
    gain_part = lax.dynamic_slice_in_dim(branch_norm_gain, column * columns, columns)
    return (residual.astype(jnp.float32) + branch * scale[:, None] * gain_part).astype(jnp.bfloat16)


def solution(mesh):
    sp_size, tp_size = mesh.shape["sp"], mesh.shape["tp"]
    sp = ("hi", "lo", "inner")
    placed = (
        P(sp, "tp"),
        P(sp, "tp"),
        P(sp, "tp"),
        P(sp, "tp"),
        P(),
        P("tp", sp),
        P(),
        P(sp, "tp"),
        P(),
        P(sp, "tp"),
    )

    def whole(*arrays):
        inner = max(1, HEAD_DIM * sp_size // arrays[7].shape[0])
        hi = sp_size // (2 * inner)
        devices = mesh.devices.reshape(hi, 2, inner, tp_size)
        paired = Mesh(devices, ("hi", "lo", "inner", "tp"))
        return jax.shard_map(
            functools.partial(per_device, hi, inner, tp_size),
            mesh=paired,
            in_specs=placed,
            out_specs=P(sp, "tp"),
            check_vma=False,
        )(*arrays)

    return whole
```

time: 212 us -> 197 us (0.929)
  Pallas kernels: 34.3 us -> 143 us
  waiting for transfers between devices: 117 us -> 18.2 us
  starting transfers between devices: 26.1 us -> 5.8 us
  local copies, waits for them, and re-layouts: 9.73 us -> 6.3 us
    pallas_call x4 -> x3, Pallas kernels: 34.3 us -> 143 us  [the longest x1 130 us: front(): pl.pallas_call(functools.partial(front_kernel, sizes), in_specs=[vmem] *...]
    ppermute x15 -> x1, waiting for transfers between devices: 116 us -> 17.5 us  [per_device(): arrived = lax.ppermute(away, 'lo', [(0, 1), (1, 0)])]
    ppermute x15 -> x1, starting transfers between devices: 26.1 us -> 5.79 us  [per_device(): arrived = lax.ppermute(away, 'lo', [(0, 1), (1, 0)])]
    dynamic_slice x1 -> x0, local copies, waits for them, and re-layouts: 2.17 us -> none  [of_parity(): lax.dynamic_index_in_dim(split, parity, axis=2, keepdims=False)]
    unnamed x32 -> x14, local copies, waits for them, and re-layouts: 6.02 us -> 5.56 us
  transfers between devices with their start and end apart: 16 -> 2, of which waited for: 11 -> 1; matrix products, arithmetic and copies ran while one was open for 2% -> 0% of each run, Pallas kernels for 16% -> 70%
where the time goes in v2:
time: 197 us; the launch traced here: 196 us
  Pallas kernels  143 us (73%)
  waiting for transfers between devices  18.2 us (9%)
  between operations  13.5 us (7%)
  local copies, waits for them, and re-layouts  6.3 us (3%)
  blocking collectives  5.88 us (3%)
  starting transfers between devices  5.8 us (3%)
  other arithmetic  3.64 us (2%)
    pallas_call x1, Pallas kernels, front(): pl.pallas_call(functools.partial(front_kernel, sizes), in_specs=[vmem] *...  130 us
    ppermute x1, waiting for transfers between devices, per_device(): arrived = lax.ppermute(away, 'lo', [(0, 1), (1, 0)])  17.5 us
    pallas_call x2, Pallas kernels, product(): pl.pallas_call(product_kernel, grid=(columns // tile,), in_specs=[pl.Bloc...  12.7 us
    psum x1, blocking collectives, per_device(): squares = lax.psum(jnp.sum(branch * branch, axis=1), 'tp')  5.88 us
    ppermute x1, starting transfers between devices, per_device(): arrived = lax.ppermute(away, 'lo', [(0, 1), (1, 0)])  5.79 us
    unnamed x14, local copies, waits for them, and re-layouts  5.56 us
  transfers between devices with their start and end apart: 2, of which 1 were waited for; matrix products, arithmetic and copies ran while one was open for 0% of the time, Pallas kernels for 70%

profile of v2, /device:TPU:24, one launch (start us, length us, event | category | flops | bytes accessed | tf_op | source)
XLA Modules:
  0.0 196.0 jit_solution(288749129470066344)
XLA Ops:
  6.5 0.0 copy-start
  6.5 0.0 all-gather.2.cloned.1.call-start
  6.5 0.7 all-gather.2.cloned.1.call-update
  7.3 0.7 reshape.12.surge_ref
  8.0 0.0 copy-done
  8.0 0.0 copy-start.1
  8.0 1.2 copy-done.1
  9.3 0.0 copy-start.2
  9.3 1.2 copy-done.2
  10.5 0.0 copy-start.3
  10.5 1.2 copy-done.3
  11.7 0.0 copy-start.4
  11.7 1.2 copy-done.4
  12.9 0.0 copy-start.5
  12.9 0.7 copy-done.5
  13.6 130.1 %front.1.parts_ref = bf16[2,4,512,512]{3,2,1,0:T(8,128)(2,1)} custom-call(bf16[512,1024]{1,0:T(8,128)(2,1)S(1)} %copy-done.1, bf16[512,1024]{1,0:T(8,128)(2,1)S(1)} %copy-done.2, bf16[512,1024]{1,0:T(8,128)(2,1)S(1)} %copy-done.3, bf16[512,1024]{1,0:T(8,128)(2,1)S(1)} %copy-done.4, f32[8,1,128]{2,1,0:T(1,128)S(1)} %constant_dynamic-slice_fusion.gap_ref, ...), custom_call_target="tpu_custom_call" | custom-call | flops 1048576000 | bytes 4194304 | tf_op jit(solution)/shard_map/front/pallas_call | solution.py:344
  143.6 0.0 all-gather.2.cloned.1.call-done.weight_ref
  143.7 6.2 %product.3 = bf16[512,1024]{1,0:T(8,128)(2,1)} custom-call(bf16[2,4,512,512]{3,2,1,0:T(8,128)(2,1)} %front.1.parts_ref, bf16[2048,1024]{1,0:T(8,128)(2,1)} %all-gather.2.cloned.1.call-done.weight_ref), custom_call_target="tpu_custom_call" | custom-call | flops 2147483648 | bytes 6291456 | tf_op jit(solution)/shard_map/product/pallas_call | solution.py:384
  149.9 5.8 %collective-permute-start = (bf16[512,1024]{1,0:T(8,128)(2,1)}, bf16[512,1024]{1,0:T(8,128)(2,1)S(1)}, u32[]{:S(2)}, u32[]{:S(2)}) collective-permute-start(bf16[512,1024]{1,0:T(8,128)(2,1)} %product.3), channel_id=1, source_target_pairs={{0,4},{4,0},{1,5},{5,1},{2,6},{6,2},{3,7},{7,3},{8,12},{12,8},{9,1... | collective-permute-start | bytes 3145736 | tf_op jit(solution)/shard_map/ppermute | solution.py:435
  155.7 6.4 %product.2 = f32[512,1024]{1,0:T(8,128)} custom-call(bf16[2,4,512,512]{3,2,1,0:T(8,128)(2,1)} %front.1.parts_ref, bf16[2048,1024]{1,0:T(8,128)(2,1)} %all-gather.2.cloned.1.call-done.weight_ref), custom_call_target="tpu_custom_call" | custom-call | flops 2147483648 | bytes 6291456 | tf_op jit(solution)/shard_map/product/pallas_call | solution.py:384
  162.1 0.0 copy-start.6
  162.1 0.0 dynamic-slice-start
  162.1 17.5 %collective-permute-done = bf16[512,1024]{1,0:T(8,128)(2,1)S(1)} collective-permute-done((bf16[512,1024]{1,0:T(8,128)(2,1)}, bf16[512,1024]{1,0:T(8,128)(2,1)S(1)}, u32[]{:S(2)}, u32[]{:S(2)}) %collective-permute-start) | collective-permute-done | bytes 1048608 | tf_op jit(solution)/shard_map/ppermute | solution.py:435
  179.6 1.9 add_convert_fusion
  181.6 0.3 fusion
  181.9 5.9 %psum.7 = f32[512]{0:T(512)S(1)} all-reduce(f32[512]{0:T(512)S(1)} %fusion), channel_id=1, replica_groups=mesh['hi'=4,'lo'=2,'inner'=1,'tp'=4] {'tp'}, use_global_device_ids=true, to_apply=%region_1.0 | all-reduce | flops 512 | bytes 4096 | tf_op jit(solution)/shard_map/psum | solution.py:439
  187.7 0.0 copy-done.6
  187.7 0.0 dynamic-slice-done
  187.7 1.4 fusion.3
  (2 shorter events, 0.0 us)
Async XLA Ops:
  6.5 1.5 copy-start
  6.5 137.1 %all-gather.2.cloned.1.call-start = ((), (), s32[]{:S(2)}) async-start(), calls=%async_computation | async-start | bytes 5242880 | tf_op jit(solution)/shard_map/all_gather | solution.py:420
  8.0 1.2 copy-start.1
  9.3 1.2 copy-start.2
  10.5 1.2 copy-start.3
  11.7 1.2 copy-start.4
  12.9 0.7 copy-start.5
  149.9 29.7 %collective-permute-start = (bf16[512,1024]{1,0:T(8,128)(2,1)}, bf16[512,1024]{1,0:T(8,128)(2,1)S(1)}, u32[]{:S(2)}, u32[]{:S(2)}) collective-permute-start(bf16[512,1024]{1,0:T(8,128)(2,1)} %product.3), channel_id=1, source_target_pairs={{0,4},{4,0},{1,5},{5,1},{2,6},{6,2},{3,7},{7,3},{8,12},{12,8},{9,1... | collective-permute-start | bytes 3145736 | tf_op jit(solution)/shard_map/ppermute | solution.py:435
  162.1 25.6 %copy-start.6 = (bf16[512,1024]{1,0:T(8,128)(2,1)S(1)}, bf16[512,1024]{1,0:T(8,128)(2,1)}, u32[]{:S(2)}) copy-start(bf16[512,1024]{1,0:T(8,128)(2,1)} %param.19) | copy-start | bytes 3145732
  162.1 25.6 %dynamic-slice-start = ((f32[4096]{0:T(1024)}, s32[]{:T(128)}), f32[1024]{0:T(1024)S(1)}, s32[]{:S(2)}) async-start(f32[4096]{0:T(1024)} %param.18, s32[]{:T(128)} %select_n.7), calls=%async_computation.1 | async-start | bytes 8704 | tf_op jit(solution)/shard_map/dynamic_slice | solution.py:442
Sparse Core Ops, SparseCore 0:
  8.9 97.4 all-gather.1

commit v3 on v2

--- a/solution.py
+++ b/solution.py
@@ -90,14 +90,17 @@
 
 def front_kernel(
     sizes,
-    query_ref,
-    forget_ref,
-    value_ref,
-    gate_ref,
+    query_in,
+    forget_in,
+    value_in,
+    gate_in,
     gap_ref,
     surge_ref,
     gain_ref,
+    weight_ref,
+    projected_ref,
     parts_ref,
+    whole_weight,
     state_out,
     total_out,
     state_in,
@@ -105,14 +108,24 @@
     carried,
     span_total,
     away,
+    query_ref,
+    forget_ref,
+    value_ref,
+    gate_ref,
+    partial_out,
+    partial_in,
+    here,
     state_sems,
     total_sems,
     swap_sems,
     tp_sems,
+    load_sems,
+    weight_sems,
+    partial_sems,
 ):
     hi_size, inner_size, tp_size, block = sizes
     sp_size = 2 * hi_size * inner_size
-    rows, width = query_ref.shape
+    rows, width = query_in.shape
     heads = width // HEAD_DIM
     half = heads // 2
     per = block // HEAD_DIM
@@ -140,8 +153,76 @@
     def flipped(stride):
         return tp + stride - 2 * stride * ((tp // stride) % 2)
 
+    line = hi_size * inner_size
+    spot = lax.axis_index("hi") * inner_size + inner
+    depth = weight_ref.shape[0]
+    pieces, _, tile = partial_out.shape
+
+    def slot(number):
+        return pl.ds(pl.multiple_of(number * depth, depth), depth)
+
+    loads = [
+        pltpu.make_async_copy(source, target, load_sems.at[number])
+        for number, (source, target) in enumerate(
+            (
+                (weight_ref, whole_weight.at[slot(spot)]),
+                (forget_in, forget_ref),
+                (value_in, value_ref),
+                (query_in, query_ref),
+                (gate_in, gate_ref),
+            )
+        )
+    ]
+    for load in loads:
+        load.start()
+
+    def on_line(position):
+        return {"hi": position // inner_size, "inner": position % inner_size}
+
+    def weight_copy(way, hop, piece):
+        step = 1 if way == 0 else -1
+        block = whole_weight.at[slot(spot - step * (hop - 1)), pl.ds(piece * tile, tile)]
+        return pltpu.make_async_remote_copy(
+            src_ref=block,
+            dst_ref=block,
+            send_sem=weight_sems.at[0, way, hop - 1, piece],
+            recv_sem=weight_sems.at[1, way, hop - 1, piece],
+            device_id=on_line(spot + step),
+            device_id_type=MESH_ID,
+        )
+
+    def sends(way, hop):
+        step = 1 if way == 0 else -1
+        origin = spot - step * (hop - 1)
+        target = spot + step
+        return (origin >= 0) & (origin < line) & (target >= 0) & (target < line)
+
+    def receives(way, hop):
+        origin = spot - (1 if way == 0 else -1) * hop
+        return (origin >= 0) & (origin < line)
+
+    def send_weight(way, hop, piece):
+        @pl.when(sends(way, hop))
+        def _():
+            weight_copy(way, hop, piece).start()
+
+    def take_weight(hop, piece):
+        for way in (0, 1):
+
+            @pl.when(receives(way, hop))
+            def _():
+                weight_copy(way, hop, piece).wait_recv()
+
+            if hop + 1 < line:
+                send_weight(way, hop + 1, piece)
+
+    def take_hop(hop):
+        for piece in range(pieces):
+            take_weight(hop, piece)
+
     barrier = pltpu.get_barrier_semaphore()
     reaches = sorted(set(shifts + [inner_size]))
+    neighbours = [spot + 1, spot - 1]
     peers = len(strides)
     for by in reaches:
         for there in (place + by, place - by):
@@ -152,11 +233,27 @@
                 pl.semaphore_signal(barrier, inc=1, device_id=at(there), device_id_type=MESH_ID)
 
             peers = peers + jnp.where(inside, 1, 0)
+    for there in neighbours:
+        inside = (there >= 0) & (there < line)
+
+        @pl.when(inside)
+        def _():
+            pl.semaphore_signal(barrier, inc=1, device_id=on_line(there), device_id_type=MESH_ID)
+
+        peers = peers + jnp.where(inside, 1, 0)
     for stride in strides:
         pl.semaphore_signal(
             barrier, inc=1, device_id={"tp": flipped(stride)}, device_id_type=MESH_ID
         )
     pl.semaphore_wait(barrier, peers)
+    loads[0].wait()
+    late = pieces // 2
+    for piece in range(pieces):
+        send_weight(1, 1, piece)
+        if piece < late:
+            send_weight(0, 1, piece)
+    loads[1].wait()
+    loads[2].wait()
 
     def lanes_of(head):
         return pl.ds(pl.multiple_of(head * HEAD_DIM, HEAD_DIM), HEAD_DIM)
@@ -192,6 +289,9 @@
             for copy in copies:
                 copy.start()
 
+        if late < pieces:
+            send_weight(0, 1, late)
+            late += 1
         if turn == 0:
 
             @pl.when(place == 0)
@@ -221,6 +321,12 @@
             state_out[turn + 1] = carried[...].astype(jnp.bfloat16)
             total_out[turn + 1] = span_total[...]
 
+    for piece in range(late, pieces):
+        send_weight(0, 1, piece)
+    if line > 1:
+        take_hop(1)
+    loads[3].wait()
+    loads[4].wait()
     gain = gain_ref[...]
 
     def compute(head, put):
@@ -293,6 +399,9 @@
 
     lax.fori_loop(0, half, own_body, 0)
 
+    if line > 2:
+        take_hop(2)
+
     for stage in range(len(strides)):
 
         def pass_body(chunk, carry):
@@ -304,6 +413,48 @@
             return carry
 
         lax.fori_loop(0, half, pass_body, 0)
+
+    for hop in range(3, line - 1):
+        take_hop(hop)
+
+    def partial_copy(piece):
+        return pltpu.make_async_remote_copy(
+            src_ref=partial_out.at[piece],
+            dst_ref=partial_in.at[piece],
+            send_sem=partial_sems.at[0, piece],
+            recv_sem=partial_sems.at[1, piece],
+            device_id={"lo": 1 - lo},
+            device_id_type=MESH_ID,
+        )
+
+    def multiplied(which, piece):
+        part_width = width // 2
+        total = None
+        for place in range(tp_size):
+            block = whole_weight[pl.ds(place * part_width, part_width), pl.ds(piece * tile, tile)]
+            term = dot(parts_ref[which, place], block)
+            total = term if total is None else total + term
+        return total
+
+    for piece in range(pieces):
+        if line > 3:
+            take_weight(line - 1, piece)
+        partial_out[piece] = multiplied(1, piece).astype(jnp.bfloat16)
+        partial_copy(piece).start()
+        here[piece] = multiplied(0, piece)
+    for piece in range(pieces):
+        partial_copy(piece).wait_recv()
+        total = here[piece] + partial_in[piece].astype(jnp.float32)
+        projected_ref[:, pl.ds(piece * tile, tile)] = total.astype(jnp.bfloat16)
+
+    for piece in range(pieces):
+        partial_copy(piece).wait_send()
+        for way in (0, 1):
+            for hop in range(1, line):
+
+                @pl.when(sends(way, hop))
+                def _():
+                    weight_copy(way, hop, piece).wait_send()
 
     for turn, by in enumerate(shifts):
 
@@ -333,20 +484,29 @@
     lax.fori_loop(0, half, sent_body, 0)
 
 
-def front(sizes, query_logits, forget_logits, value_inputs, gate_logits, gap, surge, gain):
+def front(
+    sizes, query_logits, forget_logits, value_inputs, gate_logits, gap, surge, gain, weight
+):
     hi_size, inner_size, tp_size, block = sizes
     rows, width = query_logits.shape
     heads = width // HEAD_DIM
     turns = 1 + (2 * hi_size * inner_size - 2).bit_length()
     stages = tp_size.bit_length() - 1
     vmem = pl.BlockSpec(memory_space=pltpu.VMEM)
+    anywhere = pl.BlockSpec(memory_space=pl.ANY)
     state = (heads, HEAD_DIM, HEAD_DIM)
+    line = hi_size * inner_size
+    depth, columns = weight.shape
+    tile = 256
+    pieces = columns // tile
     return pl.pallas_call(
         functools.partial(front_kernel, sizes),
-        in_specs=[vmem] * 7,
+        in_specs=[anywhere] * 4 + [vmem] * 3 + [anywhere],
         out_specs=vmem,
-        out_shape=jax.ShapeDtypeStruct((2, tp_size, rows, width // 2), jnp.bfloat16),
+        out_shape=jax.ShapeDtypeStruct((rows, columns), jnp.bfloat16),
         scratch_shapes=[
+            pltpu.VMEM((2, tp_size, rows, width // 2), jnp.bfloat16),
+            pltpu.VMEM((line * depth, columns), jnp.bfloat16),
             pltpu.VMEM((turns,) + state, jnp.bfloat16),
             pltpu.VMEM((turns, heads, 8, HEAD_DIM), jnp.float32),
             pltpu.VMEM((turns,) + state, jnp.bfloat16),
@@ -354,10 +514,20 @@
             pltpu.VMEM(state, jnp.float32),
             pltpu.VMEM((heads, 8, HEAD_DIM), jnp.float32),
             pltpu.VMEM((rows, width // 2), jnp.bfloat16),
+            pltpu.VMEM((rows, width), jnp.bfloat16),
+            pltpu.VMEM((rows, width), jnp.bfloat16),
+            pltpu.VMEM((rows, width), jnp.bfloat16),
+            pltpu.VMEM((rows, width), jnp.bfloat16),
+            pltpu.VMEM((pieces, rows, tile), jnp.bfloat16),
+            pltpu.VMEM((pieces, rows, tile), jnp.bfloat16),
+            pltpu.VMEM((pieces, rows, tile), jnp.float32),
             pltpu.SemaphoreType.DMA((2, turns)),
             pltpu.SemaphoreType.DMA((2, turns)),
             pltpu.SemaphoreType.DMA((2, heads // 2)),
             pltpu.SemaphoreType.DMA((2, stages, 2, tp_size // 2, heads // 2)),
+            pltpu.SemaphoreType.DMA((5,)),
+            pltpu.SemaphoreType.DMA((2, 2, max(1, line - 1), pieces)),
+            pltpu.SemaphoreType.DMA((2, pieces)),
         ],
         name="front",
         compiler_params=pltpu.CompilerParams(
@@ -366,37 +536,7 @@
         cost_estimate=pl.CostEstimate(
             flops=rows * width * 2000, bytes_accessed=8 * rows * width, transcendentals=0
         ),
-    )(query_logits, forget_logits, value_inputs, gate_logits, gap, surge, gain)
-
-
-def product_kernel(parts_ref, weight_ref, out_ref):
-    depth = parts_ref.shape[-1]
-    total = None
-    for place in range(parts_ref.shape[1]):
-        term = dot(parts_ref[0, place], weight_ref[pl.ds(place * depth, depth), :])
-        total = term if total is None else total + term
-    out_ref[...] = total.astype(out_ref.dtype)
-
-
-def product(which, parts, weight, dtype):
-    rows, columns = parts.shape[2], weight.shape[1]
-    tile = 256
-    return pl.pallas_call(
-        product_kernel,
-        grid=(columns // tile,),
-        in_specs=[
-            pl.BlockSpec((1,) + parts.shape[1:], lambda j: (which, 0, 0, 0)),
-            pl.BlockSpec((weight.shape[0], tile), lambda j: (0, j)),
-        ],
-        out_specs=pl.BlockSpec((rows, tile), lambda j: (0, j)),
-        out_shape=jax.ShapeDtypeStruct((rows, columns), dtype),
-        name="product",
-        cost_estimate=pl.CostEstimate(
-            flops=2 * rows * weight.shape[0] * columns,
-            bytes_accessed=2 * (weight.size + rows * weight.shape[0]),
-            transcendentals=0,
-        ),
-    )(parts, weight)
+    )(query_logits, forget_logits, value_inputs, gate_logits, gap, surge, gain, weight)
 
 
 def per_device(
@@ -417,11 +557,10 @@
     rows, width = query_logits.shape
     heads = width // HEAD_DIM
     column = lax.axis_index("tp")
-    weight = lax.all_gather(output_matrix, ("hi", "inner"), axis=0, tiled=True)
     gap = lax.dynamic_slice_in_dim(
         forget_floor_gap.reshape(-1, 1, HEAD_DIM), column * heads, heads, axis=0
     )
-    parts = front(
+    projected = front(
         (hi_size, inner_size, tp_size, inner_size * output_matrix.shape[0]),
         query_logits,
         forget_logits,
@@ -430,11 +569,8 @@
         gap,
         surge_log_decay.reshape(heads, 1, rows),
         head_norm_gain.reshape(1, HEAD_DIM),
+        output_matrix,
     )
-    away = product(1, parts, weight, jnp.bfloat16)
-    arrived = lax.ppermute(away, "lo", [(0, 1), (1, 0)])
-    here = product(0, parts, weight, jnp.float32)
-    projected = (here + arrived.astype(jnp.float32)).astype(jnp.bfloat16)
     branch = lax.optimization_barrier(projected).astype(jnp.float32)
     squares = lax.psum(jnp.sum(branch * branch, axis=1), "tp")
     columns = branch.shape[1]

time: 197 us -> 132 us (0.67)
  Pallas kernels: 143 us -> 117 us
  waiting for transfers between devices: 18.2 us -> 0 us
  between operations: 13.5 us -> 0.05 us
  starting transfers between devices: 5.8 us -> 0 us
    pallas_call x3 -> x1, Pallas kernels: 143 us -> 117 us  [front(): pl.pallas_call(functools.partial(front_kernel, sizes), in_specs=[anywhere...]
    ppermute x1 -> x0, waiting for transfers between devices: 17.5 us -> none  [per_device(): arrived = lax.ppermute(away, 'lo', [(0, 1), (1, 0)])]
    ppermute x1 -> x0, starting transfers between devices: 5.79 us -> none  [per_device(): arrived = lax.ppermute(away, 'lo', [(0, 1), (1, 0)])]
  transfers between devices with their start and end apart: 2 -> 0, of which waited for: 1 -> 0; matrix products, arithmetic and copies ran while one was open for 0% -> 0% of each run, Pallas kernels for 70% -> 0%
where the time goes in v3:
time: 132 us
  Pallas kernels  117 us (89%)
  local copies, waits for them, and re-layouts  7.01 us (5%)
  blocking collectives  6.21 us (5%)
  other arithmetic  1.7 us (1%)
    pallas_call x1, Pallas kernels, front(): pl.pallas_call(functools.partial(front_kernel, sizes), in_specs=[anywhere...  117 us
    unnamed x14, local copies, waits for them, and re-layouts  6.27 us
    psum x1, blocking collectives, per_device(): squares = lax.psum(jnp.sum(branch * branch, axis=1), 'tp')  6.21 us

profile of v3, /device:TPU:24, one launch (start us, length us, event | category | flops | bytes accessed | tf_op | source)
XLA Modules:
  0.0 131.9 jit_solution(5920112463160126859)
XLA Ops:
  0.0 0.0 copy-start
  0.0 0.7 copy-done
  0.7 0.7 reshape.12.surge_ref
  1.5 0.0 copy-start.1
  1.5 1.2 copy-done.1
  2.7 0.0 copy-start.2
  2.7 1.2 copy-done.2
  3.9 0.0 copy-start.3
  3.9 1.2 copy-done.3
  5.1 0.0 copy-start.4
  5.1 1.2 copy-done.4
  6.4 0.0 copy-start.5
  6.4 0.7 copy-done.5
  7.0 116.9 %front.1 = bf16[512,1024]{1,0:T(8,128)(2,1)S(1)} custom-call(bf16[512,1024]{1,0:T(8,128)(2,1)S(1)} %copy-done.1, bf16[512,1024]{1,0:T(8,128)(2,1)S(1)} %copy-done.2, bf16[512,1024]{1,0:T(8,128)(2,1)S(1)} %copy-done.3, bf16[512,1024]{1,0:T(8,128)(2,1)S(1)} %copy-done.4, f32[8,1,128]{2,1,0:T(1,128)S(1)} %constant_dynamic-slice_fusion.gap_ref, ...), custom_call_target="tpu_custom_call" | custom-call | flops 1048576000 | bytes 4194304 | tf_op jit(solution)/shard_map/front/pallas_call | solution.py:502
  123.9 0.0 copy-start.6
  123.9 0.0 dynamic-slice-start
  123.9 0.3 fusion
  124.2 6.2 %psum.7 = f32[512]{0:T(512)S(1)} all-reduce(f32[512]{0:T(512)S(1)} %fusion), channel_id=1, replica_groups=mesh['hi'=4,'lo'=2,'inner'=1,'tp'=4] {'tp'}, use_global_device_ids=true, to_apply=%region_1.0 | all-reduce | flops 512 | bytes 4096 | tf_op jit(solution)/shard_map/psum | solution.py:575
  130.4 0.0 copy-done.6
  130.4 0.0 dynamic-slice-done
  130.4 1.4 %fusion.3 = bf16[512,1024]{1,0:T(8,128)(2,1)} fusion(bf16[512,1024]{1,0:T(8,128)(2,1)S(1)} %front.1, bf16[512,1024]{1,0:T(8,128)(2,1)S(1)} %copy-done.6, f32[1024]{0:T(1024)S(1)} %dynamic-slice-done, f32[512]{0:T(512)S(1)} %add_rsqrt_fusion), kind=kLoop, calls=%fused_computation.5 | loop fusion | flops 3145728 | bytes 3151872 | tf_op jit(solution)/shard_map/convert_element_type | solution.py:579
  (2 shorter events, 0.0 us)
Async XLA Ops:
  0.0 0.7 copy-start
  1.5 1.2 copy-start.1
  2.7 1.2 copy-start.2
  3.9 1.2 copy-start.3
  5.1 1.2 copy-start.4
  6.4 0.7 copy-start.5
  123.9 6.5 %copy-start.6 = (bf16[512,1024]{1,0:T(8,128)(2,1)S(1)}, bf16[512,1024]{1,0:T(8,128)(2,1)}, u32[]{:S(2)}) copy-start(bf16[512,1024]{1,0:T(8,128)(2,1)} %param.19) | copy-start | bytes 3145732
  123.9 6.5 %dynamic-slice-start = ((f32[4096]{0:T(1024)}, s32[]{:T(128)}), f32[1024]{0:T(1024)S(1)}, s32[]{:S(2)}) async-start(f32[4096]{0:T(1024)} %param.18, s32[]{:T(128)} %select_n.7), calls=%async_computation | async-start | bytes 8704 | tf_op jit(solution)/shard_map/dynamic_slice | solution.py:578

commit v4 on v3

--- a/solution.py
+++ b/solution.py
@@ -181,7 +181,7 @@
 
     def weight_copy(way, hop, piece):
         step = 1 if way == 0 else -1
-        block = whole_weight.at[slot(spot - step * (hop - 1)), pl.ds(piece * tile, tile)]
+        block = whole_weight.at[slot(spot - step * (hop - 1)), pl.ds(pl.multiple_of(piece * tile, tile), tile)]
         return pltpu.make_async_remote_copy(
             src_ref=block,
             dst_ref=block,
@@ -267,6 +267,8 @@
         return carry
 
     lax.fori_loop(0, heads, state_body, 0)
+
+    hop_pieces_left = list(range(pieces))
 
     for turn, by in enumerate(shifts):
         copies = [
@@ -317,14 +319,21 @@
 
             lax.fori_loop(0, heads, merge, 0)
 
-        if turn + 1 < len(shifts):
+        if line > 1 and turn < pieces:
+            if turn + 1 < len(shifts):
+                state_out[turn + 1] = carried[...].astype(jnp.bfloat16)
+                total_out[turn + 1] = span_total[...]
+            hop_pieces_left.remove(turn)
+            take_weight(1, turn)
+        elif turn + 1 < len(shifts):
             state_out[turn + 1] = carried[...].astype(jnp.bfloat16)
             total_out[turn + 1] = span_total[...]
 
     for piece in range(late, pieces):
         send_weight(0, 1, piece)
     if line > 1:
-        take_hop(1)
+        for piece in hop_pieces_left:
+            take_weight(1, piece)
     loads[3].wait()
     loads[4].wait()
     gain = gain_ref[...]
@@ -381,6 +390,8 @@
 
         compute(head_of(chunk, 1 - lo), put)
         swap_copy(chunk).start()
+        if line > 2 and pieces == half:
+            take_weight(2, chunk)
         return carry
 
     lax.fori_loop(0, half, away_body, 0)
@@ -399,7 +410,7 @@
 
     lax.fori_loop(0, half, own_body, 0)
 
-    if line > 2:
+    if line > 2 and pieces != half:
         take_hop(2)
 
     for stage in range(len(strides)):
@@ -531,7 +542,7 @@
         ],
         name="front",
         compiler_params=pltpu.CompilerParams(
-            collective_id=0, has_side_effects=True, vmem_limit_bytes=48 * 1024 * 1024
+            collective_id=0, has_side_effects=True, vmem_limit_bytes=64000 * 1024
         ),
         cost_estimate=pl.CostEstimate(
             flops=rows * width * 2000, bytes_accessed=8 * rows * width, transcendentals=0

time: 132 us -> 147 us (1.11)
  Pallas kernels: 117 us -> 134 us
  local copies, waits for them, and re-layouts: 7.01 us -> 2.66 us
    pallas_call x1, Pallas kernels: 117 us -> 134 us  [front(): pl.pallas_call(functools.partial(front_kernel, sizes), in_specs=[anywhere...]
    unnamed x14 -> x6, local copies, waits for them, and re-layouts: 6.27 us -> 0.73 us
where the time goes in v4:
time: 147 us; the launch traced here: 146 us
  Pallas kernels  134 us (91%)
  blocking collectives  6.22 us (4%)
  other arithmetic  3.01 us (2%)
  local copies, waits for them, and re-layouts  2.66 us (2%)
    pallas_call x1, Pallas kernels, front(): pl.pallas_call(functools.partial(front_kernel, sizes), in_specs=[anywhere...  134 us
    psum x1, blocking collectives, per_device(): squares = lax.psum(jnp.sum(branch * branch, axis=1), 'tp')  6.22 us

profile of v4, /device:TPU:24, one launch (start us, length us, event | category | flops | bytes accessed | tf_op | source)
XLA Modules:
  0.0 146.4 jit_solution(719029726548140377)
XLA Ops:
  0.0 0.0 copy-start
  0.0 0.7 copy-done
  0.7 0.6 constant_dynamic-slice_fusion.gap_ref
  1.3 1.3 reshape.12.surge_ref
  2.6 0.0 copy-start.2
  2.6 134.5 %front.1 = bf16[512,1024]{1,0:T(8,128)(2,1)} custom-call(bf16[512,1024]{1,0:T(8,128)(2,1)} %query_in.1, bf16[512,1024]{1,0:T(8,128)(2,1)} %forget_in.1, bf16[512,1024]{1,0:T(8,128)(2,1)} %value_in.1, bf16[512,1024]{1,0:T(8,128)(2,1)} %gate_in.1, f32[8,1,128]{2,1,0:T(1,128)} %constant_dynamic-slice_fusion.gap_ref, f32[8,1,512]{2,1,0:T(1,128)} %reshape.12.surge_ref, ...), custom_call_target="tpu_custom_call" | custom-call | flops 1048576000 | bytes 4194304 | tf_op jit(solution)/shard_map/front/pallas_call | solution.py:513
  137.1 0.0 copy-start.1
  137.2 0.0 dynamic-slice-start
  137.2 1.6 %fusion = f32[512]{0:T(512)S(1)} fusion(bf16[512,1024]{1,0:T(8,128)(2,1)} %front.1), kind=kLoop, calls=%fused_computation.2 | loop fusion | flops 1572352 | bytes 1050624 | tf_op jit(solution)/shard_map/reduce_sum | solution.py:586
  138.8 6.2 %psum.7 = f32[512]{0:T(512)S(1)} all-reduce(f32[512]{0:T(512)S(1)} %fusion), channel_id=1, replica_groups=mesh['hi'=4,'lo'=2,'inner'=1,'tp'=4] {'tp'}, use_global_device_ids=true, to_apply=%region_1.0 | all-reduce | flops 512 | bytes 4096 | tf_op jit(solution)/shard_map/psum | solution.py:586
  145.0 0.0 copy-done.2
  145.0 0.0 copy-done.1
  145.0 0.0 dynamic-slice-done
  145.0 1.4 fusion.3
  (1 shorter events, 0.0 us)
Async XLA Ops:
  0.0 0.7 copy-start
  2.6 142.3 %copy-start.2 = (bf16[512,1024]{1,0:T(8,128)(2,1)S(1)}, bf16[512,1024]{1,0:T(8,128)(2,1)}, u32[]{:S(2)}) copy-start(bf16[512,1024]{1,0:T(8,128)(2,1)} %param.19) | copy-start | bytes 3145732
  137.1 7.8 %copy-start.1 = (bf16[512,1024]{1,0:T(8,128)(2,1)S(1)}, bf16[512,1024]{1,0:T(8,128)(2,1)}, u32[]{:S(2)}) copy-start(bf16[512,1024]{1,0:T(8,128)(2,1)} %front.1) | copy-start | bytes 3145732
  137.2 7.8 %dynamic-slice-start = ((f32[4096]{0:T(1024)}, s32[]{:T(128)}), f32[1024]{0:T(1024)S(1)}, s32[]{:S(2)}) async-start(f32[4096]{0:T(1024)} %param.18, s32[]{:T(128)} %select_n.7), calls=%async_computation | async-start | bytes 8704 | tf_op jit(solution)/shard_map/dynamic_slice | solution.py:589

commit v5 on v3

--- a/solution.py
+++ b/solution.py
@@ -140,6 +140,7 @@
         }
 
     shifts = [1]
+    passed_back = 0
     by = 1
     while by < sp_size - 1:
         shifts.append(by)
@@ -181,7 +182,7 @@
 
     def weight_copy(way, hop, piece):
         step = 1 if way == 0 else -1
-        block = whole_weight.at[slot(spot - step * (hop - 1)), pl.ds(piece * tile, tile)]
+        block = whole_weight.at[slot(spot - step * (hop - 1)), pl.ds(pl.multiple_of(piece * tile, tile), tile)]
         return pltpu.make_async_remote_copy(
             src_ref=block,
             dst_ref=block,
@@ -206,8 +207,8 @@
         def _():
             weight_copy(way, hop, piece).start()
 
-    def take_weight(hop, piece):
-        for way in (0, 1):
+    def take_weight(hop, piece, ways=(0, 1)):
+        for way in ways:
 
             @pl.when(receives(way, hop))
             def _():
@@ -320,11 +321,15 @@
         if turn + 1 < len(shifts):
             state_out[turn + 1] = carried[...].astype(jnp.bfloat16)
             total_out[turn + 1] = span_total[...]
+            if line > 1 and turn >= 1 and turn - 1 < pieces:
+                take_weight(1, turn - 1, (1,))
+                passed_back = turn
 
     for piece in range(late, pieces):
         send_weight(0, 1, piece)
     if line > 1:
-        take_hop(1)
+        for piece in range(pieces):
+            take_weight(1, piece, (0, 1) if piece >= passed_back else (0,))
     loads[3].wait()
     loads[4].wait()
     gain = gain_ref[...]
@@ -381,6 +386,8 @@
 
         compute(head_of(chunk, 1 - lo), put)
         swap_copy(chunk).start()
+        if line > 2 and pieces == half:
+            take_weight(2, chunk, (1,))
         return carry
 
     lax.fori_loop(0, half, away_body, 0)
@@ -400,7 +407,8 @@
     lax.fori_loop(0, half, own_body, 0)
 
     if line > 2:
-        take_hop(2)
+        for piece in range(pieces):
+            take_weight(2, piece, (0,) if pieces == half else (0, 1))
 
     for stage in range(len(strides)):
 
@@ -531,7 +539,7 @@
         ],
         name="front",
         compiler_params=pltpu.CompilerParams(
-            collective_id=0, has_side_effects=True, vmem_limit_bytes=48 * 1024 * 1024
+            collective_id=0, has_side_effects=True, vmem_limit_bytes=64000 * 1024
         ),
         cost_estimate=pl.CostEstimate(
             flops=rows * width * 2000, bytes_accessed=8 * rows * width, transcendentals=0

time: 132 us -> 131 us (level)
  local copies, waits for them, and re-layouts: 7.01 us -> 2.66 us
    unnamed x14 -> x6, local copies, waits for them, and re-layouts: 6.27 us -> 0.73 us
    pallas_call x1, Pallas kernels: 117 us -> 118 us  [front(): pl.pallas_call(functools.partial(front_kernel, sizes), in_specs=[anywhere...]
where the time goes in v5:
time: 131 us; the launch traced here: 130 us
  Pallas kernels  118 us (90%)
  blocking collectives  6.21 us (5%)
  other arithmetic  3.01 us (2%)
  local copies, waits for them, and re-layouts  2.66 us (2%)
    pallas_call x1, Pallas kernels, front(): pl.pallas_call(functools.partial(front_kernel, sizes), in_specs=[anywhere...  118 us
    psum x1, blocking collectives, per_device(): squares = lax.psum(jnp.sum(branch * branch, axis=1), 'tp')  6.21 us

profile of v5, /device:TPU:24, one launch (start us, length us, event | category | flops | bytes accessed | tf_op | source)
XLA Modules:
  0.0 130.3 jit_solution(8552532406833926451)
XLA Ops:
  0.0 0.0 copy-start
  0.0 0.7 copy-done
  0.7 0.6 constant_dynamic-slice_fusion.gap_ref
  1.3 1.3 %reshape.12.surge_ref = f32[8,1,512]{2,1,0:T(1,128)} reshape(f32[8,512]{1,0:T(8,128)} %param.15) | data formatting | bytes 32768 | tf_op jit(solution)/shard_map/reshape | solution.py:578
  2.6 0.0 copy-start.2
  2.6 118.4 %front.1 = bf16[512,1024]{1,0:T(8,128)(2,1)} custom-call(bf16[512,1024]{1,0:T(8,128)(2,1)} %query_in.1, bf16[512,1024]{1,0:T(8,128)(2,1)} %forget_in.1, bf16[512,1024]{1,0:T(8,128)(2,1)} %value_in.1, bf16[512,1024]{1,0:T(8,128)(2,1)} %gate_in.1, f32[8,1,128]{2,1,0:T(1,128)} %constant_dynamic-slice_fusion.gap_ref, f32[8,1,512]{2,1,0:T(1,128)} %reshape.12.surge_ref, ...), custom_call_target="tpu_custom_call" | custom-call | flops 1048576000 | bytes 4194304 | tf_op jit(solution)/shard_map/front/pallas_call | solution.py:510
  121.0 0.0 copy-start.1
  121.0 0.0 dynamic-slice-start
  121.0 1.6 %fusion = f32[512]{0:T(512)S(1)} fusion(bf16[512,1024]{1,0:T(8,128)(2,1)} %front.1), kind=kLoop, calls=%fused_computation.2 | loop fusion | flops 1572352 | bytes 1050624 | tf_op jit(solution)/shard_map/reduce_sum | solution.py:583
  122.6 6.2 %psum.7 = f32[512]{0:T(512)S(1)} all-reduce(f32[512]{0:T(512)S(1)} %fusion), channel_id=1, replica_groups=mesh['hi'=4,'lo'=2,'inner'=1,'tp'=4] {'tp'}, use_global_device_ids=true, to_apply=%region_1.0 | all-reduce | flops 512 | bytes 4096 | tf_op jit(solution)/shard_map/psum | solution.py:583
  128.9 0.0 copy-done.2
  128.9 0.0 copy-done.1
  128.9 0.0 dynamic-slice-done
  128.9 1.4 %fusion.3 = bf16[512,1024]{1,0:T(8,128)(2,1)} fusion(bf16[512,1024]{1,0:T(8,128)(2,1)S(1)} %copy-done.1, bf16[512,1024]{1,0:T(8,128)(2,1)S(1)} %copy-done.2, f32[1024]{0:T(1024)S(1)} %dynamic-slice-done, f32[512]{0:T(512)S(1)} %add_rsqrt_fusion), kind=kLoop, calls=%fused_computation.5 | loop fusion | flops 3145728 | bytes 3151872 | tf_op jit(solution)/shard_map/convert_element_type | solution.py:587
  (1 shorter events, 0.0 us)
Async XLA Ops:
  0.0 0.7 copy-start
  2.6 126.2 %copy-start.2 = (bf16[512,1024]{1,0:T(8,128)(2,1)S(1)}, bf16[512,1024]{1,0:T(8,128)(2,1)}, u32[]{:S(2)}) copy-start(bf16[512,1024]{1,0:T(8,128)(2,1)} %param.19) | copy-start | bytes 3145732
  121.0 7.8 %copy-start.1 = (bf16[512,1024]{1,0:T(8,128)(2,1)S(1)}, bf16[512,1024]{1,0:T(8,128)(2,1)}, u32[]{:S(2)}) copy-start(bf16[512,1024]{1,0:T(8,128)(2,1)} %front.1) | copy-start | bytes 3145732
  121.0 7.8 %dynamic-slice-start = ((f32[4096]{0:T(1024)}, s32[]{:T(128)}), f32[1024]{0:T(1024)S(1)}, s32[]{:S(2)}) async-start(f32[4096]{0:T(1024)} %param.18, s32[]{:T(128)} %select_n.7), calls=%async_computation | async-start | bytes 8704 | tf_op jit(solution)/shard_map/dynamic_slice | solution.py:586

commit v6 on v5

--- a/solution.py
+++ b/solution.py
@@ -140,7 +140,7 @@
         }
 
     shifts = [1]
-    passed_back = 0
+    passed_back, passed_on = 0, 0
     by = 1
     while by < sp_size - 1:
         shifts.append(by)
@@ -293,6 +293,11 @@
         if late < pieces:
             send_weight(0, 1, late)
             late += 1
+        elif line > 1:
+            for _ in range(2 if turn + 1 == len(shifts) else 1):
+                if passed_on < pieces:
+                    take_weight(1, passed_on, (0,))
+                    passed_on += 1
         if turn == 0:
 
             @pl.when(place == 0)
@@ -329,7 +334,10 @@
         send_weight(0, 1, piece)
     if line > 1:
         for piece in range(pieces):
-            take_weight(1, piece, (0, 1) if piece >= passed_back else (0,))
+            if piece >= passed_back:
+                take_weight(1, piece, (1,))
+            if piece >= passed_on:
+                take_weight(1, piece, (0,))
     loads[3].wait()
     loads[4].wait()
     gain = gain_ref[...]

time: 131 us -> 135 us (1.031)
  Pallas kernels: 118 us -> 123 us
    pallas_call x1, Pallas kernels: 118 us -> 123 us  [front(): pl.pallas_call(functools.partial(front_kernel, sizes), in_specs=[anywhere...]
where the time goes in v6:
time: 135 us
  Pallas kernels  123 us (91%)
  blocking collectives  6.22 us (5%)
  other arithmetic  3.01 us (2%)
  local copies, waits for them, and re-layouts  2.66 us (2%)
    pallas_call x1, Pallas kernels, front(): pl.pallas_call(functools.partial(front_kernel, sizes), in_specs=[anywhere...  123 us
    psum x1, blocking collectives, per_device(): squares = lax.psum(jnp.sum(branch * branch, axis=1), 'tp')  6.22 us

profile of v6, /device:TPU:24, one launch (start us, length us, event | category | flops | bytes accessed | tf_op | source)
XLA Modules:
  0.0 135.1 jit_solution(12746827759254070820)
XLA Ops:
  0.0 0.0 copy-start
  0.0 0.7 copy-done
  0.7 0.6 constant_dynamic-slice_fusion.gap_ref
  1.3 1.3 reshape.12.surge_ref
  2.6 0.0 copy-start.2
  2.6 123.2 %front.1 = bf16[512,1024]{1,0:T(8,128)(2,1)} custom-call(bf16[512,1024]{1,0:T(8,128)(2,1)} %query_in.1, bf16[512,1024]{1,0:T(8,128)(2,1)} %forget_in.1, bf16[512,1024]{1,0:T(8,128)(2,1)} %value_in.1, bf16[512,1024]{1,0:T(8,128)(2,1)} %gate_in.1, f32[8,1,128]{2,1,0:T(1,128)} %constant_dynamic-slice_fusion.gap_ref, f32[8,1,512]{2,1,0:T(1,128)} %reshape.12.surge_ref, ...), custom_call_target="tpu_custom_call" | custom-call | flops 1048576000 | bytes 4194304 | tf_op jit(solution)/shard_map/front/pallas_call | solution.py:518
  125.9 0.0 copy-start.1
  125.9 0.0 dynamic-slice-start
  125.9 1.6 %fusion = f32[512]{0:T(512)S(1)} fusion(bf16[512,1024]{1,0:T(8,128)(2,1)} %front.1), kind=kLoop, calls=%fused_computation.2 | loop fusion | flops 1572352 | bytes 1050624 | tf_op jit(solution)/shard_map/reduce_sum | solution.py:591
  127.5 6.2 %psum.7 = f32[512]{0:T(512)S(1)} all-reduce(f32[512]{0:T(512)S(1)} %fusion), channel_id=1, replica_groups=mesh['hi'=4,'lo'=2,'inner'=1,'tp'=4] {'tp'}, use_global_device_ids=true, to_apply=%region_1.0 | all-reduce | flops 512 | bytes 4096 | tf_op jit(solution)/shard_map/psum | solution.py:591
  133.7 0.0 copy-done.2
  133.7 0.0 copy-done.1
  133.7 0.0 dynamic-slice-done
  133.7 1.4 %fusion.3 = bf16[512,1024]{1,0:T(8,128)(2,1)} fusion(bf16[512,1024]{1,0:T(8,128)(2,1)S(1)} %copy-done.1, bf16[512,1024]{1,0:T(8,128)(2,1)S(1)} %copy-done.2, f32[1024]{0:T(1024)S(1)} %dynamic-slice-done, f32[512]{0:T(512)S(1)} %add_rsqrt_fusion), kind=kLoop, calls=%fused_computation.5 | loop fusion | flops 3145728 | bytes 3151872 | tf_op jit(solution)/shard_map/convert_element_type | solution.py:595
  (1 shorter events, 0.0 us)
Async XLA Ops:
  0.0 0.7 copy-start
  2.6 131.1 %copy-start.2 = (bf16[512,1024]{1,0:T(8,128)(2,1)S(1)}, bf16[512,1024]{1,0:T(8,128)(2,1)}, u32[]{:S(2)}) copy-start(bf16[512,1024]{1,0:T(8,128)(2,1)} %param.19) | copy-start | bytes 3145732
  125.9 7.8 %copy-start.1 = (bf16[512,1024]{1,0:T(8,128)(2,1)S(1)}, bf16[512,1024]{1,0:T(8,128)(2,1)}, u32[]{:S(2)}) copy-start(bf16[512,1024]{1,0:T(8,128)(2,1)} %front.1) | copy-start | bytes 3145732
  125.9 7.8 %dynamic-slice-start = ((f32[4096]{0:T(1024)}, s32[]{:T(128)}), f32[1024]{0:T(1024)S(1)}, s32[]{:S(2)}) async-start(f32[4096]{0:T(1024)} %param.18, s32[]{:T(128)} %select_n.7), calls=%async_computation | async-start | bytes 8704 | tf_op jit(solution)/shard_map/dynamic_slice | solution.py:594
